TPU v7x, 256 devices: a whole 4x4x8 slice. The times are simulated.
256 devices in a mesh: gr: 2 (over z_hi), fs: 16 (over z_lo, y), tp: 8 (over x, core).
Axes of the slice: x: 4, y: 4, z: 8 (z_hi: 2, z_lo: 4; z = z_hi * 4 + z_lo), core: 2. Of those that a mesh axis runs over, the one named last changes fastest.
Arguments:
- prompt: bfloat16 [16384, 2048], P(('gr', 'fs')), may hold values from -6 to 6
- norm_gain: float32 [2048], P(('gr', 'fs')), may hold values from 0.1 to 1.9
- gate_master: float32 [32, 2048, 1024], P(None, ('gr', 'fs'), 'tp'), may hold values from -6 to 6
- up_master: float32 [32, 2048, 1024], P(None, ('gr', 'fs'), 'tp'), may hold values from -6 to 6
- down_master: float32 [32, 2048, 1024], P(None, ('gr', 'fs'), 'tp'), may hold values from -6 to 6
- routes: int32 [16384, 2], P(('gr', 'fs')), may hold values from 0 to 31, as said below
- route_weights: float32 [16384, 2], P(('gr', 'fs')), may hold values from 0.1 to 0.9
Outputs:
- gate_ready: bfloat16 [32, 2048, 1024], P('fs', None, 'tp')
- up_ready: bfloat16 [32, 2048, 1024], P('fs', None, 'tp')
- down_ready: bfloat16 [32, 2048, 1024], P('fs', None, 'tp')
- blended: bfloat16 [16384, 2048], P(('gr', 'fs'), 'tp')
Inputs may be any that keep to these rules, and one draw needn't show every extreme that they name: `routes`: each row names 2 different experts of one group: expert // 8 is the group. In every aligned block of 512 rows (the tokens of one index of gr and fs) half of the rows choose one group, and no expert is named more than 64 times; in every block some expert is named exactly 64 times.
All inputs are finite; a program needn't handle non-finite values.
Results may differ from a plain program's by a relative error of at most 0.015.
Values may be sent and summed in bfloat16 or wider, within the bound.
A program may use at most 128 MiB of HBM per device.

v0:
```python
import jax
import jax.numpy as jnp
from jax import lax
from jax.sharding import PartitionSpec as P

D = 2048
FF = 1024


EPS = 1e-06


def in_one_piece(arrays, axis, split_dim, concat_dim, along):
    both = jnp.concatenate(arrays, axis=along)
    result, at, finished = (
        lax.all_to_all(both, axis, split_axis=split_dim, concat_axis=concat_dim, tiled=True),
        0,
        [],
    )
    for a in arrays:
        finished.append(lax.slice_in_dim(result, at, at + a.shape[along], axis=along))
        at += a.shape[along]
    return tuple(finished)


def sent_together(arrays, axis, dim, along):
    widths = [a.shape[along] for a in arrays]
    both = jnp.concatenate(arrays, axis=along)
    result = lax.all_gather(both, axis, axis=dim, tiled=True)
    return tuple(jnp.split(result, [sum(widths[:k]) for k in range(1, len(widths))], axis=along))


def grouped_exchange(shard, axis, split_dim, concat_dim, work, item_dim, out_dim):
    items = jax.tree.leaves(shard)[0].shape[item_dim]
    count = 2 if items % 2 == 0 else 1
    finished = []
    for k in range(count):
        group = jax.tree.map(
            lambda a: lax.slice_in_dim(
                a, k * (items // count), (k + 1) * (items // count), axis=item_dim
            ),
            shard,
        )
        finished.append(
            work(
                lax.all_to_all(
                    group, axis, split_axis=split_dim, concat_axis=concat_dim, tiled=True
                )
            )
        )
    return jax.tree.map(lambda *parts: jnp.concatenate(parts, axis=out_dim), *finished)


def per_device(prompt, norm_gain, gate_master, up_master, down_master, routes, route_weights):
    gate_low = (norm_gain[None, :, None] * gate_master).astype(jnp.bfloat16)
    up_low = (norm_gain[None, :, None] * up_master).astype(jnp.bfloat16)
    down_low = down_master.astype(jnp.bfloat16)
    experts = gate_low.shape[0]
    fs_count = lax.axis_size("fs")
    local_experts = experts // fs_count
    resharded = in_one_piece((gate_low, up_low, down_low), "fs", 0, 1, 2)
    gate_ready, up_ready, down_ready = sent_together(
        (resharded[0], resharded[1], resharded[2]), "gr", 1, 0
    )
    tokens = prompt.shape[0]
    capacity = tokens // 8
    prompt_wide = prompt.astype(jnp.float32)
    normed = (
        prompt_wide * lax.rsqrt(jnp.mean(prompt_wide * prompt_wide, axis=-1, keepdims=True) + EPS)
    ).astype(jnp.bfloat16)
    route_list = routes.reshape(-1)
    route_hits = (route_list[:, None] == jnp.arange(experts, dtype=jnp.int32)[None, :]).astype(
        jnp.int32
    )
    slot_rank = jnp.sum((jnp.cumsum(route_hits, axis=0) - 1) * route_hits, axis=1)
    slot_index = route_list * capacity + slot_rank
    token_of = jnp.arange(route_list.shape[0], dtype=jnp.int32) // routes.shape[1]
    slot_owner = jnp.zeros((experts * capacity,), jnp.int32).at[slot_index].set(token_of)
    outgoing = normed[slot_owner].reshape(fs_count, local_experts, capacity, normed.shape[1])

    def expert_work(arrived):
        pre_gate = jnp.einsum(
            "secd,edf->secf", arrived, gate_ready, preferred_element_type=jnp.float32
        ) * D ** (-0.5)
        pre_up = jnp.einsum(
            "secd,edf->secf", arrived, up_ready, preferred_element_type=jnp.float32
        ) * D ** (-0.5)
        hidden = (jax.nn.silu(pre_gate) * pre_up).astype(jnp.bfloat16)
        partial_value = (
            jnp.einsum("secf,edf->secd", hidden, down_ready, preferred_element_type=jnp.float32)
            * FF ** (-0.5)
        ).astype(jnp.bfloat16)
        summed = lax.psum_scatter(partial_value, "tp", scatter_dimension=3, tiled=True).astype(
            jnp.float32
        )
        return lax.all_to_all(
            summed.astype(jnp.bfloat16), "fs", split_axis=0, concat_axis=0, tiled=True
        )

    answers = grouped_exchange(outgoing, "fs", 0, 0, expert_work, 2, 2)
    answers_flat = answers.reshape(experts * capacity, answers.shape[3])
    picked = answers_flat[slot_index].reshape(tokens, routes.shape[1], answers.shape[3])
    blended = jnp.sum(picked.astype(jnp.float32) * route_weights[:, :, None], axis=1)
    return (gate_ready, up_ready, down_ready, blended.astype(jnp.bfloat16))


def solution(mesh):
    in_specs = (
        P(("gr", "fs"), None),
        P(("gr", "fs")),
        P(None, ("gr", "fs"), "tp"),
        P(None, ("gr", "fs"), "tp"),
        P(None, ("gr", "fs"), "tp"),
        P(("gr", "fs"), None),
        P(("gr", "fs"), None),
    )
    out_specs = (
        P("fs", None, "tp"),
        P("fs", None, "tp"),
        P("fs", None, "tp"),
        P(("gr", "fs"), "tp"),
    )
    return jax.shard_map(
        per_device, mesh=mesh, in_specs=in_specs, out_specs=out_specs, check_vma=False
    )
```

profile of v0, /device:TPU:1, one launch (start us, length us, event | category | flops | bytes accessed | tf_op | source)
XLA Modules:
  0.0 404.5 jit_solution(14247513782647689321)
XLA Ops:
  7.2 1.3 convert_element_type.53
  8.5 1.9 multiply_convert_fusion.3
  10.4 1.4 pad_maximum_fusion
  11.8 9.2 %all-to-all-start = ((bf16[32,64,384]{2,1,0:T(8,128)(2,1)}), bf16[32,64,384]{2,1,0:T(8,128)(2,1)}, u32[]{:S(2)}, u32[]{:S(2)}) async-start(bf16[32,64,384]{2,1,0:T(8,128)(2,1)} %pad_maximum_fusion), calls=%async_computation | async-start | bytes 3145728 | tf_op jit(solution)/shard_map/all_to_all | solution.py:16
  21.1 0.1 copy.25
  21.2 0.2 eq.29
  21.4 0.2 eq.25
  21.5 0.1 copy.24
  21.7 0.2 mul.105
  21.9 9.0 %reduce-window.6 = s32[32,8,128]{2,1,0:T(8,128)S(1)} reduce-window(s32[32,8,128]{2,1,0:T(8,128)S(1)} %fusion.76, s32[]{:T(128)} %constant.37.clone.1), window={size=1x1x128 pad=0_0x0_0x127_0}, to_apply=%region_1.0 | reduce-window | flops 4161536 | bytes 262148 | tf_op jit(solution)/shard_map/reduce-window
  30.9 0.1 slice.35
  31.0 0.1 copy.27
  31.2 0.1 copy.28
  31.3 0.1 add_add_fusion
  31.4 4.3 %scatter_custom_fusion = s32[2048]{0:T(1024)S(1)} fusion(s32[1024]{0:T(1024)S(1)} %bitcast.75, s32[1024]{0:T(1024)S(1)} %add_select_fusion, s32[]{:T(128)} %constant.37.clone.1), kind=kCustom, calls=%fused_computation.73 | custom fusion | bytes 8196 | tf_op jit(solution)/shard_map/scatter | solution.py:78
  35.8 0.5 fusion
  36.3 2.0 fusion.1
  38.3 11.0 %gather_fusion = bf16[2048,2048]{1,0:T(8,128)(2,1)} fusion(bf16[512,2048]{1,0:T(8,128)(2,1)S(1)} %fusion.1, s32[2048]{0:T(1024)S(1)} %fusion.77), kind=kCustom, calls=%fused_computation | custom fusion | bytes 16785408 | tf_op jit(solution)/shard_map/gather | solution.py:79
  49.3 6.0 %fusion.87 = (bf16[16,2,32,2048]{3,2,1,0:T(8,128)(2,1)}, bf16[16,2,32,2048]{3,2,1,0:T(8,128)(2,1)}) fusion(bf16[16,2,64,2048]{3,2,1,0:T(8,128)(2,1)} %bitcast.69), kind=kLoop, calls=%fused_computation.83 | loop fusion | bytes 16777216 | tf_op jit(solution)/shard_map/slice | solution.py:39
  55.3 7.2 %all-to-all-start.3 = ((bf16[16,2,32,2048]{3,2,1,0:T(8,128)(2,1)}), bf16[16,2,32,2048]{3,2,1,0:T(8,128)(2,1)}, u32[]{:S(2)}, u32[]{:S(2)}) async-start(bf16[16,2,32,2048]{3,2,1,0:T(8,128)(2,1)} %get-tuple-element.5), calls=%async_computation.4 | async-start | bytes 8388608 | tf_op jit(solution)/shard_map/all_to_all | solution.py:46
  62.4 0.0 all-gather.2.cloned.1.call-start
  62.5 1.6 copy.23
  64.1 0.3 fusion.89
  64.3 1.3 pad_maximum_fusion.1
  65.7 0.0 all-gather.2.cloned.1.call-update
  65.7 123.5 %all-gather.2.cloned.1.call-done = bf16[6,2048,128]{2,1,0:T(8,128)(2,1)} async-done(((bf16[6,1024,128]{2,1,0:T(8,128)(2,1)}), bf16[6,2048,128]{2,1,0:T(8,128)(2,1)}) %all-gather.2.cloned.1.call-update) | async-done | bytes 3145744 | tf_op jit(solution)/shard_map/all_gather | solution.py:29
  189.2 2.1 fusion.88
  191.3 16.7 %all-to-all-done.3 = bf16[16,2,32,2048]{3,2,1,0:T(8,128)(2,1)} async-done(((bf16[16,2,32,2048]{3,2,1,0:T(8,128)(2,1)}), bf16[16,2,32,2048]{3,2,1,0:T(8,128)(2,1)}, u32[]{:S(2)}, u32[]{:S(2)}) %all-to-all-start.3) | async-done | bytes 4194336 | tf_op jit(solution)/shard_map/all_to_all | solution.py:46
  208.1 19.5 %all-to-all-start.1 = ((bf16[16,2,32,2048]{3,2,1,0:T(8,128)(2,1)}), bf16[16,2,32,2048]{3,2,1,0:T(8,128)(2,1)}, u32[]{:S(2)}, u32[]{:S(2)}) async-start(bf16[16,2,32,2048]{3,2,1,0:T(8,128)(2,1)} %get-tuple-element.4), calls=%async_computation.1 | async-start | bytes 8388608 | tf_op jit(solution)/shard_map/all_to_all | solution.py:46
  227.5 0.0 reduce-scatter.5.cloned.1.call-start
  227.6 4.2 %fusion.30 = f32[16,2,32,128]{3,2,0,1:T(8,128)} fusion(bf16[16,2,32,2048]{3,2,1,0:T(8,128)(2,1)} %all-to-all-done.3, bf16[2,2048,128]{2,1,0:T(8,128)(2,1)S(1)} %get-tuple-element.8), kind=kOutput, calls=%fused_computation.27 | convolution fusion | flops 537001984 | bytes 5767168 | tf_op jit(solution)/shard_map/secd,edf->secf/dot_general | solution.py:82
  231.8 6.6 %fusion.11 = bf16[16,2,32,2048]{3,2,0,1:T(8,128)(2,1)} fusion(bf16[16,2,32,2048]{3,2,1,0:T(8,128)(2,1)} %all-to-all-done.3, bf16[2,2048,128]{2,1,0:T(8,128)(2,1)S(1)} %get-tuple-element.7, bf16[2,2048,128]{2,1,0:T(8,128)(2,1)S(1)} %get-tuple-element.6, f32[16,2,32,128]{3,2,0,1:T(8,128)} %fusion.30), kind=kOutput, calls=%fused_computation.18 | convolution fusion | flops 1078853632 | bytes 11010048 | tf_op jit(solution)/shard_map/secf,edf->secd/dot_general | solution.py:90
  238.5 0.2 reduce-scatter.3.cloned.1.call-start
  238.7 67.1 %all-to-all-done.1 = bf16[16,2,32,2048]{3,2,1,0:T(8,128)(2,1)} async-done(((bf16[16,2,32,2048]{3,2,1,0:T(8,128)(2,1)}), bf16[16,2,32,2048]{3,2,1,0:T(8,128)(2,1)}, u32[]{:S(2)}, u32[]{:S(2)}) %all-to-all-start.1) | async-done | bytes 4194336 | tf_op jit(solution)/shard_map/all_to_all | solution.py:46
  305.8 4.3 %fusion.15 = f32[16,2,32,128]{3,2,0,1:T(8,128)} fusion(bf16[16,2,32,2048]{3,2,1,0:T(8,128)(2,1)} %all-to-all-done.1, bf16[2,2048,128]{2,1,0:T(8,128)(2,1)S(1)} %get-tuple-element.8), kind=kOutput, calls=%fused_computation.22 | convolution fusion | flops 537001984 | bytes 5767168 | tf_op jit(solution)/shard_map/secd,edf->secf/dot_general | solution.py:82
  310.1 6.6 %fusion.10 = bf16[16,2,32,2048]{3,2,0,1:T(8,128)(2,1)} fusion(bf16[16,2,32,2048]{3,2,1,0:T(8,128)(2,1)} %all-to-all-done.1, bf16[2,2048,128]{2,1,0:T(8,128)(2,1)S(1)} %get-tuple-element.7, bf16[2,2048,128]{2,1,0:T(8,128)(2,1)S(1)} %get-tuple-element.6, f32[16,2,32,128]{3,2,0,1:T(8,128)} %fusion.15), kind=kOutput, calls=%fused_computation.17 | convolution fusion | flops 1078853632 | bytes 11010048 | tf_op jit(solution)/shard_map/secf,edf->secd/dot_general | solution.py:90
  316.7 0.0 reduce-scatter.5.cloned.1.call-done
  316.8 1.9 copy.34
  318.6 19.4 %all-to-all-start.4 = ((bf16[16,2,32,256]{3,2,1,0:T(8,128)(2,1)}), bf16[16,2,32,256]{3,2,1,0:T(8,128)(2,1)S(1)}, u32[]{:S(2)}, u32[]{:S(2)}) async-start(bf16[16,2,32,256]{3,2,1,0:T(8,128)(2,1)} %copy.34), calls=%async_computation.6 | async-start | bytes 1048576 | tf_op jit(solution)/shard_map/all_to_all | solution.py:96
  338.1 32.2 %reduce-scatter.3.cloned.1.call-done = bf16[16,2,32,256]{3,2,0,1:T(8,128)(2,1)} async-done(((bf16[16,2,32,2048]{3,2,0,1:T(8,128)(2,1)}), bf16[16,2,32,256]{3,2,0,1:T(8,128)(2,1)}) %reduce-scatter.3.cloned.1.call-update) | async-done | bytes 524304 | tf_op jit(solution)/shard_map/reduce_scatter | solution.py:93
  370.3 1.9 copy.31
  372.2 6.5 %all-to-all-start.2 = ((bf16[16,2,32,256]{3,2,1,0:T(8,128)(2,1)}), bf16[16,2,32,256]{3,2,1,0:T(8,128)(2,1)S(1)}, u32[]{:S(2)}, u32[]{:S(2)}) async-start(bf16[16,2,32,256]{3,2,1,0:T(8,128)(2,1)} %copy.31), calls=%async_computation.3 | async-start | bytes 1048576 | tf_op jit(solution)/shard_map/all_to_all | solution.py:96
  378.7 0.1 copy.35
  378.9 11.0 %all-to-all-done.2 = bf16[16,2,32,256]{3,2,1,0:T(8,128)(2,1)S(1)} async-done(((bf16[16,2,32,256]{3,2,1,0:T(8,128)(2,1)}), bf16[16,2,32,256]{3,2,1,0:T(8,128)(2,1)S(1)}, u32[]{:S(2)}, u32[]{:S(2)}) %all-to-all-start.2) | async-done | bytes 524320 | tf_op jit(solution)/shard_map/all_to_all | solution.py:96
  389.8 0.1 pad_maximum_fusion.2
  389.9 3.9 gather_fusion.1
  393.9 0.5 reshape.78
  394.4 3.6 multiply_reduce_fusion
  (26 shorter events, 0.2 us)
Async XLA Ops:
  8.5 12.6 %copy-start.4 = (s32[512,2]{0,1:T(2,128)S(1)}, s32[512,2]{0,1:T(2,128)}, u32[]{:S(2)}) copy-start(s32[512,2]{0,1:T(2,128)} %param.12) | copy-start | bytes 12292
  10.4 25.4 %copy-start = (bf16[512,2048]{1,0:T(8,128)(2,1)S(1)}, bf16[512,2048]{1,0:T(8,128)(2,1)}, u32[]{:S(2)}) copy-start(bf16[512,2048]{1,0:T(8,128)(2,1)} %param.7) | copy-start | bytes 6291460
  11.8 43.5 %all-to-all-start = ((bf16[32,64,384]{2,1,0:T(8,128)(2,1)}), bf16[32,64,384]{2,1,0:T(8,128)(2,1)}, u32[]{:S(2)}, u32[]{:S(2)}) async-start(bf16[32,64,384]{2,1,0:T(8,128)(2,1)} %pad_maximum_fusion), calls=%async_computation | async-start | bytes 3145728 | tf_op jit(solution)/shard_map/all_to_all | solution.py:16
  55.3 152.8 %all-to-all-start.3 = ((bf16[16,2,32,2048]{3,2,1,0:T(8,128)(2,1)}), bf16[16,2,32,2048]{3,2,1,0:T(8,128)(2,1)}, u32[]{:S(2)}, u32[]{:S(2)}) async-start(bf16[16,2,32,2048]{3,2,1,0:T(8,128)(2,1)} %get-tuple-element.5), calls=%async_computation.4 | async-start | bytes 8388608 | tf_op jit(solution)/shard_map/all_to_all | solution.py:46
  62.4 126.8 %all-gather.2.cloned.1.call-start = ((), (), s32[]{:S(2)}) async-start(), calls=%async_computation.7 | async-start | bytes 4718592 | tf_op jit(solution)/shard_map/all_gather | solution.py:29
  191.3 114.5 %copy-start.3 = (bf16[2,2048,128]{2,1,0:T(8,128)(2,1)}, bf16[2,2048,128]{2,1,0:T(8,128)(2,1)S(1)}, u32[]{:S(2)}) copy-start(bf16[2,2048,128]{2,1,0:T(8,128)(2,1)S(1)} %get-tuple-element.8) | copy-start | bytes 3145732
  191.3 118.8 %copy-start.1 = (bf16[2,2048,128]{2,1,0:T(8,128)(2,1)}, bf16[2,2048,128]{2,1,0:T(8,128)(2,1)S(1)}, u32[]{:S(2)}) copy-start(bf16[2,2048,128]{2,1,0:T(8,128)(2,1)S(1)} %get-tuple-element.6) | copy-start | bytes 3145732
  191.3 118.8 %copy-start.2 = (bf16[2,2048,128]{2,1,0:T(8,128)(2,1)}, bf16[2,2048,128]{2,1,0:T(8,128)(2,1)S(1)}, u32[]{:S(2)}) copy-start(bf16[2,2048,128]{2,1,0:T(8,128)(2,1)S(1)} %get-tuple-element.7) | copy-start | bytes 3145732
  208.1 97.7 %all-to-all-start.1 = ((bf16[16,2,32,2048]{3,2,1,0:T(8,128)(2,1)}), bf16[16,2,32,2048]{3,2,1,0:T(8,128)(2,1)}, u32[]{:S(2)}, u32[]{:S(2)}) async-start(bf16[16,2,32,2048]{3,2,1,0:T(8,128)(2,1)} %get-tuple-element.4), calls=%async_computation.1 | async-start | bytes 8388608 | tf_op jit(solution)/shard_map/all_to_all | solution.py:46
  227.5 89.2 %reduce-scatter.5.cloned.1.call-start = ((), (), s32[]{:S(2)}) async-start(), calls=%async_computation.9 | async-start | bytes 4718592 | tf_op jit(solution)/shard_map/reduce_scatter | solution.py:93
  238.5 131.8 %reduce-scatter.3.cloned.1.call-start = ((), (), s32[]{:S(2)}) async-start(), calls=%async_computation.8 | async-start | bytes 4718592 | tf_op jit(solution)/shard_map/reduce_scatter | solution.py:93
  316.7 62.0 %copy-start.5 = (f32[512,2]{0,1:T(2,128)S(1)}, f32[512,2]{0,1:T(2,128)}, u32[]{:S(2)}) copy-start(f32[512,2]{0,1:T(2,128)} %param.13) | copy-start | bytes 12292
  318.6 53.5 %all-to-all-start.4 = ((bf16[16,2,32,256]{3,2,1,0:T(8,128)(2,1)}), bf16[16,2,32,256]{3,2,1,0:T(8,128)(2,1)S(1)}, u32[]{:S(2)}, u32[]{:S(2)}) async-start(bf16[16,2,32,256]{3,2,1,0:T(8,128)(2,1)} %copy.34), calls=%async_computation.6 | async-start | bytes 1048576 | tf_op jit(solution)/shard_map/all_to_all | solution.py:96
  372.2 17.7 %all-to-all-start.2 = ((bf16[16,2,32,256]{3,2,1,0:T(8,128)(2,1)}), bf16[16,2,32,256]{3,2,1,0:T(8,128)(2,1)S(1)}, u32[]{:S(2)}, u32[]{:S(2)}) async-start(bf16[16,2,32,256]{3,2,1,0:T(8,128)(2,1)} %copy.31), calls=%async_computation.3 | async-start | bytes 1048576 | tf_op jit(solution)/shard_map/all_to_all | solution.py:96
Sparse Core Ops, SparseCore 0:
  65.8 123.3 all-gather.1
  238.6 40.0 reduce-scatter.4
  316.8 53.3 reduce-scatter.2
where the time goes:
time: 409 us; the launch traced here: 405 us
  waiting for transfers between devices  251 us (61%)
  starting transfers between devices  62.1 us (15%)
  local copies, waits for them, and re-layouts  34.7 us (8%)
  matrix products  21.7 us (5%)
  other arithmetic  21.3 us (5%)
  between operations  14 us (3%)
    all_gather x1, waiting for transfers between devices, sent_together(): result = lax.all_gather(both, axis, axis=dim, tiled=True)  124 us
    all_to_all x2, waiting for transfers between devices, grouped_exchange(): lax.all_to_all(group, axis, split_axis=split_dim, concat_axis=concat_dim,...  83.8 us
    reduce_scatter x2, waiting for transfers between devices, expert_work(): lax.psum_scatter(partial_value, 'tp', scatter_dimension=3, tiled=True)  32.2 us
    all_to_all x2, starting transfers between devices, grouped_exchange(): lax.all_to_all(group, axis, split_axis=split_dim, concat_axis=concat_dim,...  26.6 us
    all_to_all x2, starting transfers between devices, expert_work(): lax.all_to_all(summed.astype(jnp.bfloat16), 'fs', split_axis=0, concat_ax...  25.9 us
    dot_general x2, matrix products, expert_work(): jnp.einsum('secf,edf->secd', hidden, down_ready, preferred_element_type=j...  13.2 us
    all_to_all x2, waiting for transfers between devices, expert_work(): lax.all_to_all(summed.astype(jnp.bfloat16), 'fs', split_axis=0, concat_ax...  11 us
    gather x1, local copies, waits for them, and re-layouts, per_device(): normed[slot_owner]  11 us
  transfers between devices with their start and end apart: 8, of which 5 were waited for; matrix products, arithmetic and copies ran while one was open for 16% of the time, Pallas kernels for 0%

commit v1 on v0

v1 whole, which is shorter than its diff:
```python
import jax
import jax.numpy as jnp
from jax import lax
from jax.experimental import pallas as pl
from jax.experimental.pallas import tpu as pltpu
from jax.sharding import PartitionSpec as P

MESH = pl.DeviceIdType.MESH
EPS = 1e-06
BF = jnp.bfloat16
F32 = jnp.float32

PLANES = ((0, 0, 0, 64), (1, 1, 0, 64), (2, -1, 0, 64), (3, 2, 0, 32), (3, -2, 32, 64))
TOK0, TOK1, HID0, HID1 = 0, 1, 2, 3
OWN_R, OWN_L, OWN_C, FAR_R, FAR_L, C_L, C_R, C_F0, C_F1 = range(9)


def kernel(
    prompt_hbm,
    gain_ref,
    gate_hbm,
    up_hbm,
    down_hbm,
    routes_ref,
    rw_ref,
    gate_out,
    up_out,
    down_out,
    blend_out,
    prompt_v,
    gate_v,
    up_v,
    down_v,
    stage_gu,
    stage_d,
    w_gu,
    w_d,
    slots_x,
    tok,
    hid,
    dx,
    outs,
    ans,
    s0,
    s1,
    acc,
    blend_v,
    load_sem,
    store_sem,
    wsend,
    wrecv,
    tsend,
    trecv,
    asend,
    arecv,
    dsend,
    drecv,
    rsend,
    rrecv,
):
    g = lax.axis_index("gr")
    f = lax.axis_index("fs")
    t = lax.axis_index("tp")
    me = g * 16 + f
    z = g * 4 + f // 4
    y = lax.rem(f, 4)
    x = t // 2
    c = lax.rem(t, 2)

    def at_zy(zz, yy):
        zz = lax.rem(zz + 16, 8)
        yy = lax.rem(yy + 8, 4)
        return zz // 4, lax.rem(zz, 4) * 4 + yy

    right = (g, f, lax.rem(x + 1, 4) * 2 + c)
    left = (g, f, lax.rem(x + 3, 4) * 2 + c)
    other = (g, f, x * 2 + 1 - c)
    t_l = lax.rem(x + 3, 4) * 2 + c
    t_r = lax.rem(x + 1, 4) * 2 + c
    t_f = lax.rem(x + 2, 4) * 2 + c

    loads = [
        pltpu.make_async_copy(down_hbm, down_v, load_sem.at[0]),
        pltpu.make_async_copy(prompt_hbm, prompt_v, load_sem.at[1]),
        pltpu.make_async_copy(gate_hbm, gate_v, load_sem.at[2]),
        pltpu.make_async_copy(up_hbm, up_v, load_sem.at[3]),
    ]
    for ld in loads:
        ld.start()

    barrier = pltpu.get_barrier_semaphore()

    def greet_zy(i, carry):
        gg, ff = at_zy(z + i // 4, y + lax.rem(i, 4))
        pl.semaphore_signal(barrier, inc=1, device_id=(gg, ff, t), device_id_type=MESH)
        return carry

    lax.fori_loop(1, 32, greet_zy, 0)

    def greet_tp(i, carry):
        pl.semaphore_signal(barrier, inc=1, device_id=(g, f, lax.rem(t + i, 8)), device_id_type=MESH)
        return carry

    lax.fori_loop(1, 8, greet_tp, 0)

    eye = lax.broadcasted_iota(jnp.int32, (64, 64), 0) == lax.broadcasted_iota(jnp.int32, (64, 64), 1)
    gain = jnp.sum(jnp.where(eye, gain_ref[...], 0.0), axis=1, keepdims=True)

    def round_d(p):
        def body(i, carry):
            stage_d[p, i] = down_v[i, p].astype(BF)
            return carry

        lax.fori_loop(0, 16, body, 0)
        w_d[p, me] = stage_d[p, f]

    def round_gu(p):
        def body(i, carry):
            stage_gu[p, i, :, 0:128] = (gain * gate_v[i, p]).astype(BF)
            stage_gu[p, i, :, 128:256] = (gain * up_v[i, p]).astype(BF)
            return carry

        lax.fori_loop(0, 16, body, 0)
        w_gu[p, me] = stage_gu[p, f]

    def send_w(stage, dest, p, sem):
        def body(i, carry):
            gg, ff = at_zy(z + i // 4, y + lax.rem(i, 4))
            pltpu.make_async_remote_copy(
                src_ref=stage.at[p, ff],
                dst_ref=dest.at[p, me],
                send_sem=wsend.at[sem],
                recv_sem=wrecv.at[sem],
                device_id=(gg, ff, t),
                device_id_type=MESH,
            ).start()
            return carry

        lax.fori_loop(1, 32, body, 0)

    def await_w(sems, dest, p, sem):
        part = dest.at[p, pl.ds(0, 31)]
        pltpu.make_async_copy(part, part, sems.at[sem]).wait()

    def copy_to(ref, sems, i, where):
        return pltpu.make_async_remote_copy(
            src_ref=ref,
            dst_ref=ref,
            send_sem=asend.at[sems, i],
            recv_sem=arecv.at[sems, i],
            device_id=where,
            device_id_type=MESH,
        )

    def piece(kind, tt, half):
        p = kind % 2
        if kind < 2:
            ref = tok.at[p, tt]
            return ref if half is None else ref.at[pl.ds(8 * half, 8)]
        ref = hid.at[p, tt]
        return ref if half is None else ref.at[pl.ds(512 * half, 512)]

    def ag_own(kind):
        ref = piece(kind, t, None)
        copy_to(ref, kind, OWN_R, right).start()
        copy_to(ref, kind, OWN_L, left).start()
        copy_to(ref, kind, OWN_C, other).start()

    def ag_relay(kind):
        copy_to(piece(kind, t_l, None), kind, OWN_R, right).wait_recv()
        copy_to(piece(kind, t_l, 0), kind, FAR_R, right).start()
        copy_to(piece(kind, t_l, None), kind, C_L, other).start()
        copy_to(piece(kind, t_r, None), kind, OWN_L, left).wait_recv()
        copy_to(piece(kind, t_r, 1), kind, FAR_L, left).start()
        copy_to(piece(kind, t_r, None), kind, C_R, other).start()

    def ag_far(kind):
        copy_to(piece(kind, t_f, 0), kind, FAR_R, right).wait_recv()
        copy_to(piece(kind, t_f, 0), kind, C_F0, other).start()
        copy_to(piece(kind, t_f, 1), kind, FAR_L, left).wait_recv()
        copy_to(piece(kind, t_f, 1), kind, C_F1, other).start()

    def ag_end(kind):
        for i, half in ((OWN_C, None), (C_L, None), (C_R, None), (C_F0, 0), (C_F1, 1)):
            copy_to(piece(kind, t, half), kind, i, other).wait_recv()

    def ag_drain(kind):
        for i, half in (
            (OWN_R, None),
            (OWN_L, None),
            (OWN_C, None),
            (FAR_R, 0),
            (FAR_L, 1),
            (C_L, None),
            (C_R, None),
            (C_F0, 0),
            (C_F1, 1),
        ):
            copy_to(piece(kind, t, half), kind, i, other).wait_send()

    def send_tokens(p):
        for j, dz, lo, hi in PLANES:
            for dy in range(4):
                gg, ff = at_zy(z + dz, y + dy)
                if dz == 0 and dy == 0:
                    continue
                pltpu.make_async_remote_copy(
                    src_ref=slots_x.at[p, ff, pl.ds(lo, hi - lo)],
                    dst_ref=tok.at[p, t, j * 4 + y, pl.ds(lo, hi - lo)],
                    send_sem=tsend.at[p],
                    recv_sem=trecv.at[p],
                    device_id=(gg, ff, t),
                    device_id_type=MESH,
                ).start()
        tok[p, t, y] = slots_x[p, f]

    def await_tokens(sems, p):
        part = slots_x.at[p, pl.ds(0, 15)]
        pltpu.make_async_copy(part, part, sems.at[p]).wait()

    def send_back(p):
        for j, dz, lo, hi in PLANES:
            for dy in range(4):
                if dz == 0 and dy == 0:
                    continue
                gg, ff = at_zy(z - dz, y + dy)
                pltpu.make_async_remote_copy(
                    src_ref=outs.at[p, j * 4 + lax.rem(y + dy, 4), pl.ds(lo, hi - lo)],
                    dst_ref=ans.at[p, f, pl.ds(lo, hi - lo)],
                    send_sem=rsend.at[p],
                    recv_sem=rrecv.at[p],
                    device_id=(gg, ff, t),
                    device_id_type=MESH,
                ).start()
        ans[p, f] = outs[p, y]

    def await_back(sems, p):
        part = outs.at[p, pl.ds(0, 15)]
        pltpu.make_async_copy(part, part, sems.at[p]).wait()

    def send_dx(p):
        def body(i, carry):
            tt = lax.rem(t + i, 8)
            pltpu.make_async_remote_copy(
                src_ref=w_d.at[p, pl.ds(tt * 4, 4)],
                dst_ref=dx.at[p, t],
                send_sem=dsend.at[p],
                recv_sem=drecv.at[p],
                device_id=(g, f, tt),
                device_id_type=MESH,
            ).start()
            return carry

        lax.fori_loop(1, 8, body, 0)
        dx[p, t] = w_d[p, pl.ds(t * 4, 4)]

    def await_dx(sems, p):
        part = dx.at[p, pl.ds(0, 7)]
        pltpu.make_async_copy(part, part, sems.at[p]).wait()

    def hidden(p):
        def body(r, carry):
            rows = jnp.concatenate(
                [tok[p, tt, pl.ds(r * 4, 4)].reshape(256, 256) for tt in range(8)], axis=1
            )
            pre = jnp.dot(rows, w_gu[p].reshape(2048, 256), preferred_element_type=F32) * 2048 ** (-0.5)
            gate, up = pre[:, 0:128], pre[:, 128:256]
            value = gate / (1.0 + jnp.exp(-gate)) * up
            hid[p, t, pl.ds(r * 256, 256)] = value.astype(BF)
            return carry

        lax.fori_loop(0, 4, body, 0)

    def expert_out(p):
        def body(r, carry):
            rows = jnp.concatenate([hid[p, tt, pl.ds(r * 256, 256)] for tt in range(8)], axis=1)
            cols = jnp.concatenate([dx[p, tt].reshape(256, 128) for tt in range(8)], axis=1)
            value = lax.dot_general(rows, cols, (((1,), (1,)), ((), ())), preferred_element_type=F32)
            value = (value * 1024 ** (-0.5)).astype(BF)
            outs[p, pl.ds(r * 4, 4)] = value.reshape(4, 64, 256)
            return carry

        lax.fori_loop(0, 4, body, 0)

    def blend(p):
        for r in range(2):
            rows = pl.ds(r * 256, 256)
            values = ans[p].reshape(1024, 256)
            first = jnp.dot(s0[p, rows], values, preferred_element_type=F32)
            second = jnp.dot(s1[p, rows], values, preferred_element_type=F32)
            part = rw_ref[rows, 0:1] * first + rw_ref[rows, 1:2] * second
            if p == 0:
                acc[rows] = part
            else:
                blend_v[rows] = (acc[rows] + part).astype(BF)

    loads[0].wait()
    round_d(0)
    pl.semaphore_wait(barrier, 38)
    send_w(stage_d, w_d, 0, 0)

    lanes = lax.broadcasted_iota(jnp.int32, (512, 128), 1)
    hit0 = jnp.where(routes_ref[:, 0:1] == lanes, 1.0, 0.0)
    hit1 = jnp.where(routes_ref[:, 1:2] == lanes, 1.0, 0.0)
    row_i = lax.broadcasted_iota(jnp.int32, (512, 512), 0)
    col_i = lax.broadcasted_iota(jnp.int32, (512, 512), 1)
    before = jnp.where(col_i < row_i, 1.0, 0.0).astype(BF)
    rank0 = jnp.dot(before, hit0.astype(BF), preferred_element_type=F32)
    rank1 = jnp.dot(before, hit1.astype(BF), preferred_element_type=F32) + jnp.sum(hit0, axis=0, keepdims=True)
    place = ((lanes >> 1) * 64 + (lanes & 1) * 1024).astype(F32)
    slot0 = jnp.sum((rank0 + place) * hit0, axis=1, keepdims=True)
    slot1 = jnp.sum((rank1 + place) * hit1, axis=1, keepdims=True)
    diag = col_i == row_i
    slot0_row = jnp.sum(jnp.where(diag, slot0, 0.0), axis=0, keepdims=True)
    slot1_row = jnp.sum(jnp.where(diag, slot1, 0.0), axis=0, keepdims=True)

    loads[1].wait()
    wide = prompt_v[...].astype(F32)
    scale = lax.rsqrt(jnp.sum(wide * wide, axis=1, keepdims=True) * (1.0 / 2048) + EPS)
    mine = prompt_v[:, pl.ds(pl.multiple_of(t * 256, 256), 256)].astype(F32)
    normed = (mine * scale).astype(BF)
    for p in range(2):
        for r in range(4):
            number = (lax.broadcasted_iota(jnp.int32, (256, 512), 0) + (p * 1024 + r * 256)).astype(F32)
            pick = jnp.where((number == slot0_row) | (number == slot1_row), 1.0, 0.0).astype(BF)
            rows = jnp.dot(pick, normed, preferred_element_type=F32).astype(BF)
            slots_x[p, pl.ds(r * 4, 4)] = rows.reshape(4, 64, 256)
        send_tokens(p)

    loads[2].wait()
    loads[3].wait()
    round_gu(0)
    send_w(stage_gu, w_gu, 0, 2)
    round_gu(1)
    send_w(stage_gu, w_gu, 1, 3)
    round_d(1)
    for p in range(2):
        number = (lax.broadcasted_iota(jnp.int32, (512, 1024), 1) + p * 1024).astype(F32)
        s0[p] = jnp.where(number == slot0, 1.0, 0.0).astype(BF)
        s1[p] = jnp.where(number == slot1, 1.0, 0.0).astype(BF)

    await_tokens(trecv, 0)
    ag_own(TOK0)
    await_tokens(trecv, 1)
    ag_own(TOK1)
    ag_relay(TOK0)
    ag_relay(TOK1)
    await_w(wrecv, w_d, 0, 0)
    send_dx(0)
    stores = []

    def store(src, dst, i):
        cp = pltpu.make_async_copy(src, dst, store_sem.at[i])
        cp.start()
        stores.append(cp)

    store(w_d.at[0], down_out.at[0], 0)
    ag_far(TOK0)
    ag_end(TOK0)
    await_w(wrecv, w_gu, 0, 2)
    hidden(0)
    ag_own(HID0)
    store(w_gu.at[0, :, :, pl.ds(0, 128)], gate_out.at[0], 1)
    store(w_gu.at[0, :, :, pl.ds(128, 128)], up_out.at[0], 2)
    ag_far(TOK1)
    ag_relay(HID0)
    ag_far(HID0)
    await_dx(drecv, 0)
    ag_end(HID0)
    expert_out(0)
    send_back(0)
    send_w(stage_d, w_d, 1, 1)
    ag_end(TOK1)
    await_w(wrecv, w_gu, 1, 3)
    hidden(1)
    ag_own(HID1)
    store(w_gu.at[1, :, :, pl.ds(0, 128)], gate_out.at[1], 3)
    store(w_gu.at[1, :, :, pl.ds(128, 128)], up_out.at[1], 4)
    ag_relay(HID1)
    ag_far(HID1)
    ag_end(HID1)
    await_back(rrecv, 0)
    blend(0)
    await_w(wrecv, w_d, 1, 1)
    send_dx(1)
    store(w_d.at[1], down_out.at[1], 5)
    await_dx(drecv, 1)
    expert_out(1)
    send_back(1)
    for kind in range(4):
        ag_drain(kind)
    for p in range(2):
        await_w(wsend, w_d, p, p)
        await_w(wsend, w_gu, p, 2 + p)
        await_tokens(tsend, p)
        await_dx(dsend, p)
    await_back(rsend, 0)
    await_back(rrecv, 1)
    blend(1)
    store(blend_v, blend_out, 6)
    await_back(rsend, 1)
    for cp in stores:
        cp.wait()


def per_device(prompt, norm_gain, gate_master, up_master, down_master, routes, route_weights):
    any_spec = pl.BlockSpec(memory_space=pl.ANY)
    vmem = pl.BlockSpec(memory_space=pltpu.VMEM)
    ready = jax.ShapeDtypeStruct((2, 32, 64, 128), BF)
    dma = pltpu.SemaphoreType.DMA
    split = lambda a: a.reshape(16, 2, 64, 128)
    gate, up, down, out = pl.pallas_call(
        kernel,
        out_shape=(ready, ready, ready, jax.ShapeDtypeStruct((512, 256), BF)),
        in_specs=[any_spec, vmem, any_spec, any_spec, any_spec, vmem, vmem],
        out_specs=(any_spec,) * 4,
        scratch_shapes=[
            pltpu.VMEM((512, 2048), BF),
            pltpu.VMEM((16, 2, 64, 128), F32),
            pltpu.VMEM((16, 2, 64, 128), F32),
            pltpu.VMEM((16, 2, 64, 128), F32),
            pltpu.VMEM((2, 16, 64, 256), BF),
            pltpu.VMEM((2, 16, 64, 128), BF),
            pltpu.VMEM((2, 32, 64, 256), BF),
            pltpu.VMEM((2, 32, 64, 128), BF),
            pltpu.VMEM((2, 16, 64, 256), BF),
            pltpu.VMEM((2, 8, 16, 64, 256), BF),
            pltpu.VMEM((2, 8, 1024, 128), BF),
            pltpu.VMEM((2, 8, 4, 64, 128), BF),
            pltpu.VMEM((2, 16, 64, 256), BF),
            pltpu.VMEM((2, 16, 64, 256), BF),
            pltpu.VMEM((2, 512, 1024), BF),
            pltpu.VMEM((2, 512, 1024), BF),
            pltpu.VMEM((512, 256), F32),
            pltpu.VMEM((512, 256), BF),
            dma((4,)),
            dma((7,)),
            dma((4,)),
            dma((4,)),
            dma((2,)),
            dma((2,)),
            dma((4, 9)),
            dma((4, 9)),
            dma((2,)),
            dma((2,)),
            dma((2,)),
            dma((2,)),
        ],
        compiler_params=pltpu.CompilerParams(
            collective_id=0, has_side_effects=True, vmem_limit_bytes=56 * 2**20
        ),
    )(
        prompt,
        norm_gain.reshape(1, 64),
        split(gate_master),
        split(up_master),
        split(down_master),
        routes,
        route_weights,
    )
    flat = lambda a: a.reshape(2, 2048, 128)
    return flat(gate), flat(up), flat(down), out


def solution(mesh):
    in_specs = (
        P(("gr", "fs"), None),
        P(("gr", "fs")),
        P(None, ("gr", "fs"), "tp"),
        P(None, ("gr", "fs"), "tp"),
        P(None, ("gr", "fs"), "tp"),
        P(("gr", "fs"), None),
        P(("gr", "fs"), None),
    )
    out_specs = (
        P("fs", None, "tp"),
        P("fs", None, "tp"),
        P("fs", None, "tp"),
        P(("gr", "fs"), "tp"),
    )
    return jax.shard_map(
        per_device, mesh=mesh, in_specs=in_specs, out_specs=out_specs, check_vma=False
    )
```

time: 409 us -> 137 us (0.33); the launches traced: 405 us -> 137 us
  waiting for transfers between devices: 251 us -> 0 us
  Pallas kernels: 0 us -> 128 us
  starting transfers between devices: 62.1 us -> 0 us
  local copies, waits for them, and re-layouts: 34.7 us -> 8.14 us
  matrix products: 21.7 us -> 0 us
  other arithmetic: 21.3 us -> 0 us
  between operations: 14 us -> 0.66 us
    pallas_call x0 -> x1, Pallas kernels: none -> 128 us  [per_device(): pl.pallas_call(kernel, out_shape=(ready, ready, ready, jax.ShapeDtypeStru...]
    all_gather x1 -> x0, waiting for transfers between devices: 124 us -> none  [sent_together(): result = lax.all_gather(both, axis, axis=dim, tiled=True)]
    all_to_all x5 -> x0, waiting for transfers between devices: 94.8 us -> none  [the longest x2 83.8 us: grouped_exchange(): lax.all_to_all(group, axis, split_axis=split_dim, concat_axis=concat_dim,...]
    all_to_all x5 -> x0, starting transfers between devices: 61.8 us -> none  [the longest x2 26.6 us: grouped_exchange(): lax.all_to_all(group, axis, split_axis=split_dim, concat_axis=concat_dim,...]
    reduce_scatter x2 -> x0, waiting for transfers between devices: 32.2 us -> none  [expert_work(): lax.psum_scatter(partial_value, 'tp', scatter_dimension=3, tiled=True)]
    dot_general x4 -> x0, matrix products: 21.7 us -> none  [the longest x2 13.2 us: expert_work(): jnp.einsum('secf,edf->secd', hidden, down_ready, preferred_element_type=j...]
    gather x2 -> x0, local copies, waits for them, and re-layouts: 14.9 us -> none  [the longest x1 11 us: per_device(): normed[slot_owner]]
    another operation x2 -> x0, other arithmetic: 9.04 us -> none
  transfers between devices with their start and end apart: 8 -> 0, of which waited for: 5 -> 0; matrix products, arithmetic and copies ran while one was open for 16% -> 0% of each run, Pallas kernels for 0% -> 0%
where the time goes in v1:
time: 137 us
  Pallas kernels  128 us (93%)
  local copies, waits for them, and re-layouts  8.14 us (6%)
    pallas_call x1, Pallas kernels, per_device(): pl.pallas_call(kernel, out_shape=(ready, ready, ready, jax.ShapeDtypeStru...  128 us
    unnamed x12, local copies, waits for them, and re-layouts  8.14 us

profile of v1, /device:TPU:1, one launch (start us, length us, event | category | flops | bytes accessed | tf_op | source)
XLA Modules:
  0.0 136.9 jit_solution(13869480572330729041)
XLA Ops:
  0.6 1.5 %copy.11.routes_ref = s32[512,2]{1,0:T(8,128)} copy(s32[512,2]{0,1:T(2,128)} %param.12) | data formatting | bytes 8192 | tf_op args[5]
  2.2 1.5 %copy.12.rw_ref = f32[512,2]{1,0:T(8,128)} copy(f32[512,2]{0,1:T(2,128)} %param.13) | data formatting | bytes 8192 | tf_op args[6]
  3.7 128.1 %shard_map.102 = (bf16[2,32,64,128]{3,2,1,0:T(8,128)(2,1)}, bf16[2,32,64,128]{3,2,1,0:T(8,128)(2,1)}, bf16[2,32,64,128]{3,2,1,0:T(8,128)(2,1)}, bf16[512,256]{1,0:T(8,128)(2,1)}) custom-call(bf16[512,2048]{1,0:T(8,128)(2,1)} %prompt_hbm.1, f32[1,64]{1,0:T(1,128)} %bitcast.13, f32[16,2,64,128]{3,2,1,0:T(8,128)} %bitcast.10, f32[16,2,64,128]{3,2,1,0:T(8,128)} %bitcast.11, ...), custom_call_target="tpu_custom_call" | custom-call | tf_op jit(solution)/shard_map/pallas_call | solution.py:412
  131.8 0.0 copy-start.1
  131.9 0.0 copy-start
  131.9 2.4 %copy.17 = bf16[2,2048,128]{2,1,0:T(8,128)(2,1)} copy(bf16[2,2048,128]{2,1,0:T(8,128)(2,1)} %bitcast.9) | data formatting | bytes 2097152
  134.3 0.0 copy-done.1
  134.3 0.0 copy-start.2
  134.3 1.0 copy.18
  135.3 0.0 copy-done
  135.3 1.0 copy.19
  136.2 0.0 copy-done.2
  136.2 0.7 copy.20
Async XLA Ops:
  131.8 2.4 %copy-start.1 = (bf16[2,32,64,128]{3,2,1,0:T(8,128)(2,1)S(1)}, bf16[2,32,64,128]{3,2,1,0:T(8,128)(2,1)}, u32[]{:S(2)}) copy-start(bf16[2,32,64,128]{3,2,1,0:T(8,128)(2,1)} %get-tuple-element.9) | copy-start | bytes 3145732
  131.9 3.4 %copy-start = (bf16[2,32,64,128]{3,2,1,0:T(8,128)(2,1)S(1)}, bf16[2,32,64,128]{3,2,1,0:T(8,128)(2,1)}, u32[]{:S(2)}) copy-start(bf16[2,32,64,128]{3,2,1,0:T(8,128)(2,1)} %get-tuple-element.10) | copy-start | bytes 3145732
  134.3 1.9 %copy-start.2 = (bf16[512,256]{1,0:T(8,128)(2,1)S(1)}, bf16[512,256]{1,0:T(8,128)(2,1)}, u32[]{:S(2)}) copy-start(bf16[512,256]{1,0:T(8,128)(2,1)} %get-tuple-element.19) | copy-start | bytes 786436

commit v2 on v1

v2 whole, which is shorter than its diff:
```python
import jax
import jax.numpy as jnp
from jax import lax
from jax.experimental import pallas as pl
from jax.experimental.pallas import tpu as pltpu
from jax.sharding import PartitionSpec as P

MESH = pl.DeviceIdType.MESH
EPS = 1e-06
BF = jnp.bfloat16
F32 = jnp.float32

PLANES = ((0, 0, 0, 64), (1, 1, 0, 64), (2, -1, 0, 64), (3, 2, 0, 32), (3, -2, 32, 64))
TOK0, TOK1, HID0, HID1 = 0, 1, 2, 3
OWN_R, OWN_L, OWN_C, FAR_R, FAR_L, C_L, C_R, C_F0, C_F1 = range(9)


def kernel(
    prompt_hbm,
    gain_hbm,
    gate_hbm,
    up_hbm,
    down_hbm,
    routes_hbm,
    rw_hbm,
    w_gu0,
    w_gu1,
    w_d,
    blend_v,
    gain_ref,
    routes_ref,
    rw_ref,
    prompt_v,
    gate_v,
    up_v,
    down_v,
    stage_gu,
    stage_d,
    slots_x,
    tok,
    hid,
    dx,
    outs,
    ans,
    s0,
    s1,
    acc,
    load_sem,
    wsend,
    wrecv,
    tsend,
    trecv,
    asend,
    arecv,
    dsend,
    drecv,
    rsend,
    rrecv,
):
    w_gu = (w_gu0, w_gu1)
    g = lax.axis_index("gr")
    f = lax.axis_index("fs")
    t = lax.axis_index("tp")
    me = g * 16 + f
    z = g * 4 + f // 4
    y = lax.rem(f, 4)
    x = t // 2
    c = lax.rem(t, 2)

    def at_zy(zz, yy):
        zz = lax.rem(zz + 16, 8)
        yy = lax.rem(yy + 8, 4)
        return zz // 4, lax.rem(zz, 4) * 4 + yy

    right = (g, f, lax.rem(x + 1, 4) * 2 + c)
    left = (g, f, lax.rem(x + 3, 4) * 2 + c)
    other = (g, f, x * 2 + 1 - c)
    t_l = lax.rem(x + 3, 4) * 2 + c
    t_r = lax.rem(x + 1, 4) * 2 + c
    t_f = lax.rem(x + 2, 4) * 2 + c

    barrier = pltpu.get_barrier_semaphore()

    def greet_zy(i, carry):
        gg, ff = at_zy(z + i // 4, y + lax.rem(i, 4))
        pl.semaphore_signal(barrier, inc=1, device_id=(gg, ff, t), device_id_type=MESH)
        return carry

    lax.fori_loop(1, 32, greet_zy, 0)

    def greet_tp(i, carry):
        pl.semaphore_signal(barrier, inc=1, device_id=(g, f, lax.rem(t + i, 8)), device_id_type=MESH)
        return carry

    lax.fori_loop(1, 8, greet_tp, 0)

    loads = [
        pltpu.make_async_copy(routes_hbm, routes_ref, load_sem.at[0]),
        pltpu.make_async_copy(prompt_hbm, prompt_v, load_sem.at[1]),
        pltpu.make_async_copy(gate_hbm, gate_v, load_sem.at[2]),
        pltpu.make_async_copy(up_hbm, up_v, load_sem.at[3]),
        pltpu.make_async_copy(down_hbm, down_v, load_sem.at[4]),
        pltpu.make_async_copy(gain_hbm, gain_ref, load_sem.at[5]),
        pltpu.make_async_copy(rw_hbm, rw_ref, load_sem.at[6]),
    ]
    for ld in loads:
        ld.start()

    def round_d(p):
        def body(i, carry):
            stage_d[p, i] = down_v[i, p].astype(BF)
            return carry

        lax.fori_loop(0, 16, body, 0)
        w_d[p, me] = stage_d[p, f]

    def round_gu(p, gain):
        def body(i, carry):
            stage_gu[p, i, :, 0:128] = (gain * gate_v[i, p]).astype(BF)
            stage_gu[p, i, :, 128:256] = (gain * up_v[i, p]).astype(BF)
            return carry

        lax.fori_loop(0, 16, body, 0)
        w_gu[p][me] = stage_gu[p, f]

    def send_w(stage, dest, sem, rows):
        def body(i, carry):
            gg, ff = at_zy(z + i // 4, y + lax.rem(i, 4))
            pltpu.make_async_remote_copy(
                src_ref=stage.at[ff, rows],
                dst_ref=dest.at[me, rows],
                send_sem=wsend.at[sem],
                recv_sem=wrecv.at[sem],
                device_id=(gg, ff, t),
                device_id_type=MESH,
            ).start()
            return carry

        lax.fori_loop(1, 32, body, 0)

    def await_w(sems, dest, sem, rows):
        part = dest.at[pl.ds(0, 31), rows]
        pltpu.make_async_copy(part, part, sems.at[sem]).wait()

    def copy_to(ref, sems, i, where):
        return pltpu.make_async_remote_copy(
            src_ref=ref,
            dst_ref=ref,
            send_sem=asend.at[sems, i],
            recv_sem=arecv.at[sems, i],
            device_id=where,
            device_id_type=MESH,
        )

    def piece(kind, tt, half):
        p = kind % 2
        if kind < 2:
            ref = tok.at[p, tt]
            return ref if half is None else ref.at[pl.ds(8 * half, 8)]
        ref = hid.at[p, tt]
        return ref if half is None else ref.at[pl.ds(512 * half, 512)]

    def ag_own(kind):
        ref = piece(kind, t, None)
        copy_to(ref, kind, OWN_R, right).start()
        copy_to(ref, kind, OWN_L, left).start()
        copy_to(ref, kind, OWN_C, other).start()

    def ag_relay(kind):
        copy_to(piece(kind, t_l, None), kind, OWN_R, right).wait_recv()
        copy_to(piece(kind, t_l, 0), kind, FAR_R, right).start()
        copy_to(piece(kind, t_l, None), kind, C_L, other).start()
        copy_to(piece(kind, t_r, None), kind, OWN_L, left).wait_recv()
        copy_to(piece(kind, t_r, 1), kind, FAR_L, left).start()
        copy_to(piece(kind, t_r, None), kind, C_R, other).start()

    def ag_far(kind):
        copy_to(piece(kind, t_f, 0), kind, FAR_R, right).wait_recv()
        copy_to(piece(kind, t_f, 0), kind, C_F0, other).start()
        copy_to(piece(kind, t_f, 1), kind, FAR_L, left).wait_recv()
        copy_to(piece(kind, t_f, 1), kind, C_F1, other).start()

    def ag_end(kind):
        for i, half in ((OWN_C, None), (C_L, None), (C_R, None), (C_F0, 0), (C_F1, 1)):
            copy_to(piece(kind, t, half), kind, i, other).wait_recv()

    def ag_drain(kind):
        for i, half in (
            (OWN_R, None),
            (OWN_L, None),
            (OWN_C, None),
            (FAR_R, 0),
            (FAR_L, 1),
            (C_L, None),
            (C_R, None),
            (C_F0, 0),
            (C_F1, 1),
        ):
            copy_to(piece(kind, t, half), kind, i, other).wait_send()

    def send_tokens(p):
        for j, dz, lo, hi in PLANES:
            for dy in range(4):
                gg, ff = at_zy(z + dz, y + dy)
                if dz == 0 and dy == 0:
                    continue
                pltpu.make_async_remote_copy(
                    src_ref=slots_x.at[p, ff, pl.ds(lo, hi - lo)],
                    dst_ref=tok.at[p, t, j * 4 + y, pl.ds(lo, hi - lo)],
                    send_sem=tsend.at[p],
                    recv_sem=trecv.at[p],
                    device_id=(gg, ff, t),
                    device_id_type=MESH,
                ).start()
        tok[p, t, y] = slots_x[p, f]

    def await_tokens(sems, p):
        part = slots_x.at[p, pl.ds(0, 15)]
        pltpu.make_async_copy(part, part, sems.at[p]).wait()

    def send_back(p, plane, sem, lanes):
        for j, dz, lo, hi in PLANES:
            for dy in range(4):
                if j != plane or (dz == 0 and dy == 0):
                    continue
                gg, ff = at_zy(z - dz, y + dy)
                pltpu.make_async_remote_copy(
                    src_ref=outs.at[p, j * 4 + lax.rem(y + dy, 4), pl.ds(lo, hi - lo), lanes],
                    dst_ref=ans.at[p, f, pl.ds(lo, hi - lo), lanes],
                    send_sem=rsend.at[sem],
                    recv_sem=rrecv.at[sem],
                    device_id=(gg, ff, t),
                    device_id_type=MESH,
                ).start()
        if plane == 0:
            ans[p, f, :, lanes] = outs[p, y, :, lanes]

    def await_back(sems, p, sem, lanes):
        part = outs.at[p, pl.ds(0, 15), :, lanes]
        pltpu.make_async_copy(part, part, sems.at[sem]).wait()

    def send_dx(p, h):
        def body(i, carry):
            tt = lax.rem(t + i, 8)
            pltpu.make_async_remote_copy(
                src_ref=w_d.at[p, pl.ds(tt * 4, 4), pl.ds(32 * h, 32)],
                dst_ref=dx.at[p, h, t],
                send_sem=dsend.at[p, h],
                recv_sem=drecv.at[p, h],
                device_id=(g, f, tt),
                device_id_type=MESH,
            ).start()
            return carry

        lax.fori_loop(1, 8, body, 0)
        dx[p, h, t] = w_d[p, pl.ds(t * 4, 4), pl.ds(32 * h, 32)]

    def await_dx(sems, p, h):
        part = dx.at[p, h, pl.ds(0, 7)]
        pltpu.make_async_copy(part, part, sems.at[p, h]).wait()

    def hidden(p):
        def body(r, carry):
            rows = jnp.concatenate(
                [tok[p, tt, pl.ds(r * 4, 4)].reshape(256, 256) for tt in range(8)], axis=1
            )
            pre = jnp.dot(rows, w_gu[p][...].reshape(2048, 256), preferred_element_type=F32) * 2048 ** (-0.5)
            gate, up = pre[:, 0:128], pre[:, 128:256]
            value = gate / (1.0 + jnp.exp(-gate)) * up
            hid[p, t, pl.ds(r * 256, 256)] = value.astype(BF)
            return carry

        lax.fori_loop(0, 4, body, 0)

    def expert_out(p, halves, sem, lanes):
        for r in (3, 1, 2, 0):
            rows = jnp.concatenate([hid[p, tt, pl.ds(r * 256, 256)] for tt in range(8)], axis=1)
            cols = jnp.concatenate(
                [
                    jnp.concatenate([dx[p, h, tt].reshape(128, 128) for tt in range(8)], axis=1)
                    for h in halves
                ],
                axis=0,
            )
            value = lax.dot_general(rows, cols, (((1,), (1,)), ((), ())), preferred_element_type=F32)
            value = (value * 1024 ** (-0.5)).astype(BF)
            outs[p, pl.ds(r * 4, 4), :, lanes] = value.reshape(4, 64, 128 * len(halves))
            send_back(p, r, sem, lanes)

    def blend(p, lanes):
        for r in range(2):
            rows = pl.ds(r * 256, 256)
            here = slice(r * 256, r * 256 + 256)
            values = ans[p, :, :, lanes].reshape(1024, lanes.size)
            first = jnp.dot(s0[p, rows], values, preferred_element_type=F32)
            second = jnp.dot(s1[p, rows], values, preferred_element_type=F32)
            part = rw0[here] * first + rw1[here] * second
            if p == 0:
                acc[rows] = part
            else:
                acc[rows, lanes] += part

    def place_columns():
        a = lax.broadcasted_iota(jnp.int32, (256, 256), 0)
        b = lax.broadcasted_iota(jnp.int32, (256, 256), 1)
        goes = a == ((b >> 5) & 1) * 128 + (b >> 6) * 32 + (b & 31)
        to_place = jnp.where(goes, 1.0, 0.0).astype(BF)
        blend_v[...] = jnp.dot(acc[...].astype(BF), to_place, preferred_element_type=F32).astype(BF)

    whole = pl.ds(0, 256)
    low, high = pl.ds(0, 128), pl.ds(128, 128)
    all_rows = pl.ds(0, 64)
    rows_a, rows_b = pl.ds(0, 32), pl.ds(32, 32)

    loads[0].wait()
    row_i = lax.broadcasted_iota(jnp.int32, (512, 512), 0)
    col_i = lax.broadcasted_iota(jnp.int32, (512, 512), 1)
    diag = col_i == row_i

    def column(row):
        return jnp.sum(jnp.where(diag, row, 0.0), axis=1, keepdims=True)

    experts = lax.broadcasted_iota(jnp.int32, (32, 512), 0)
    hit0 = jnp.where(routes_ref[0:1] == experts, 1.0, 0.0)
    hit1 = jnp.where(routes_ref[1:2] == experts, 1.0, 0.0)
    before = jnp.where(row_i < col_i, 1.0, 0.0).astype(BF)
    rank0 = jnp.dot(hit0.astype(BF), before, preferred_element_type=F32)
    rank1 = jnp.dot(hit1.astype(BF), before, preferred_element_type=F32) + jnp.sum(hit0, axis=1, keepdims=True)
    place = ((experts >> 1) * 64 + (experts & 1) * 1024).astype(F32)
    slot0_row = jnp.sum((rank0 + place) * hit0, axis=0, keepdims=True)
    slot1_row = jnp.sum((rank1 + place) * hit1, axis=0, keepdims=True)

    loads[1].wait()
    wide = prompt_v[...].astype(F32)
    scale = lax.rsqrt(jnp.sum(wide * wide, axis=1, keepdims=True) * (1.0 / 2048) + EPS)
    mine = prompt_v[:, pl.ds(pl.multiple_of(t * 256, 256), 256)].astype(F32)
    normed = (mine * scale).astype(BF)

    def pick_slots(p):
        for r in range(4):
            number = (lax.broadcasted_iota(jnp.int32, (256, 512), 0) + (p * 1024 + r * 256)).astype(F32)
            pick = jnp.where((number == slot0_row) | (number == slot1_row), 1.0, 0.0).astype(BF)
            rows = jnp.dot(pick, normed, preferred_element_type=F32).astype(BF)
            slots_x[p, pl.ds(r * 4, 4)] = rows.reshape(4, 64, 256)

    pick_slots(0)
    pick_slots(1)
    loads[4].wait()
    round_d(0)
    pl.semaphore_wait(barrier, 38)
    send_tokens(0)
    send_tokens(1)
    send_w(stage_d.at[0], w_d.at[0], 0, all_rows)
    loads[2].wait()
    loads[3].wait()
    loads[5].wait()
    eye = lax.broadcasted_iota(jnp.int32, (64, 64), 0) == lax.broadcasted_iota(jnp.int32, (64, 64), 1)
    gain = jnp.sum(jnp.where(eye, gain_ref[...], 0.0), axis=1, keepdims=True)
    round_gu(0, gain)
    send_w(stage_gu.at[0], w_gu0, 2, all_rows)
    round_gu(1, gain)
    send_w(stage_gu.at[1], w_gu1, 3, all_rows)
    round_d(1)
    send_w(stage_d.at[1], w_d.at[1], 1, rows_a)
    await_tokens(trecv, 0)
    ag_own(TOK0)
    await_tokens(trecv, 1)
    ag_own(TOK1)
    slot0 = column(slot0_row)
    slot1 = column(slot1_row)
    for p in range(2):
        number = (lax.broadcasted_iota(jnp.int32, (512, 1024), 1) + p * 1024).astype(F32)
        s0[p] = jnp.where(number == slot0, 1.0, 0.0).astype(BF)
        s1[p] = jnp.where(number == slot1, 1.0, 0.0).astype(BF)
    loads[6].wait()
    rw0 = column(rw_ref[0:1])
    rw1 = column(rw_ref[1:2])
    ag_relay(TOK0)
    ag_relay(TOK1)
    ag_far(TOK0)
    ag_far(TOK1)
    ag_end(TOK0)
    ag_end(TOK1)
    await_w(wrecv, w_d.at[0], 0, all_rows)
    send_dx(0, 0)
    send_dx(0, 1)
    await_w(wrecv, w_gu0, 2, all_rows)
    hidden(0)
    ag_own(HID0)
    ag_relay(HID0)
    ag_far(HID0)
    await_dx(drecv, 0, 0)
    await_dx(drecv, 0, 1)
    ag_end(HID0)
    expert_out(0, (0, 1), 0, whole)
    send_w(stage_d.at[1], w_d.at[1], 4, rows_b)
    await_w(wrecv, w_gu1, 3, all_rows)
    hidden(1)
    ag_own(HID1)
    ag_relay(HID1)
    ag_far(HID1)
    await_w(wrecv, w_d.at[1], 1, rows_a)
    send_dx(1, 0)
    ag_end(HID1)
    await_back(rrecv, 0, 0, whole)
    blend(0, whole)
    await_w(wrecv, w_d.at[1], 4, rows_b)
    send_dx(1, 1)
    await_dx(drecv, 1, 0)
    expert_out(1, (0,), 1, low)
    await_dx(drecv, 1, 1)
    expert_out(1, (1,), 2, high)
    for kind in range(4):
        ag_drain(kind)
    for p in range(2):
        await_tokens(tsend, p)
        for h in range(2):
            await_dx(dsend, p, h)
    await_w(wsend, w_d.at[0], 0, all_rows)
    await_w(wsend, w_d.at[1], 1, rows_a)
    await_w(wsend, w_gu0, 2, all_rows)
    await_w(wsend, w_gu1, 3, all_rows)
    await_w(wsend, w_d.at[1], 4, rows_b)
    await_back(rsend, 0, 0, whole)
    await_back(rrecv, 1, 1, low)
    blend(1, low)
    await_back(rrecv, 1, 2, high)
    blend(1, high)
    place_columns()
    await_back(rsend, 1, 1, low)
    await_back(rsend, 1, 2, high)


def copy_out(w_gu0, w_gu1, w_d, blend_v, gate_out, up_out, down_out, blend_out, sem):
    copies = [
        pltpu.make_async_copy(w_gu0.at[:, :, pl.ds(0, 128)], gate_out.at[0], sem.at[0]),
        pltpu.make_async_copy(w_gu1.at[:, :, pl.ds(0, 128)], gate_out.at[1], sem.at[1]),
        pltpu.make_async_copy(w_gu0.at[:, :, pl.ds(128, 128)], up_out.at[0], sem.at[2]),
        pltpu.make_async_copy(w_gu1.at[:, :, pl.ds(128, 128)], up_out.at[1], sem.at[3]),
        pltpu.make_async_copy(w_d, down_out, sem.at[4]),
        pltpu.make_async_copy(blend_v, blend_out, sem.at[5]),
    ]
    for cp in copies:
        cp.start()
    for cp in copies:
        cp.wait()


def per_device(prompt, norm_gain, gate_master, up_master, down_master, routes, route_weights):
    hbm = pl.BlockSpec(memory_space=pltpu.HBM)
    vmem = pl.BlockSpec(memory_space=pltpu.VMEM)
    ready = jax.ShapeDtypeStruct((2, 32, 64, 128), BF)
    both = jax.ShapeDtypeStruct((32, 64, 256), BF)
    block = jax.ShapeDtypeStruct((512, 256), BF)
    dma = pltpu.SemaphoreType.DMA
    split = lambda a: a.reshape(16, 2, 64, 128)
    w_gu0, w_gu1, w_d, out = pl.pallas_call(
        kernel,
        out_shape=(both, both, ready, block),
        in_specs=[hbm] * 7,
        out_specs=(vmem,) * 4,
        scratch_shapes=[
            pltpu.VMEM((1, 64), F32),
            pltpu.VMEM((2, 512), jnp.int32),
            pltpu.VMEM((2, 512), F32),
            pltpu.VMEM((512, 2048), BF),
            pltpu.VMEM((16, 2, 64, 128), F32),
            pltpu.VMEM((16, 2, 64, 128), F32),
            pltpu.VMEM((16, 2, 64, 128), F32),
            pltpu.VMEM((2, 16, 64, 256), BF),
            pltpu.VMEM((2, 16, 64, 128), BF),
            pltpu.VMEM((2, 16, 64, 256), BF),
            pltpu.VMEM((2, 8, 16, 64, 256), BF),
            pltpu.VMEM((2, 8, 1024, 128), BF),
            pltpu.VMEM((2, 2, 8, 4, 32, 128), BF),
            pltpu.VMEM((2, 16, 64, 256), BF),
            pltpu.VMEM((2, 16, 64, 256), BF),
            pltpu.VMEM((2, 512, 1024), BF),
            pltpu.VMEM((2, 512, 1024), BF),
            pltpu.VMEM((512, 256), F32),
            dma((7,)),
            dma((5,)),
            dma((5,)),
            dma((2,)),
            dma((2,)),
            dma((4, 9)),
            dma((4, 9)),
            dma((2, 2)),
            dma((2, 2)),
            dma((3,)),
            dma((3,)),
        ],
        compiler_params=pltpu.CompilerParams(
            collective_id=0, has_side_effects=True, vmem_limit_bytes=50 * 2**20
        ),
    )(
        prompt,
        norm_gain.reshape(1, 64),
        split(gate_master),
        split(up_master),
        split(down_master),
        routes.T,
        route_weights.T,
    )
    gate, up, down, out = pl.pallas_call(
        copy_out,
        out_shape=(ready, ready, ready, block),
        in_specs=[vmem] * 4,
        out_specs=(hbm,) * 4,
        scratch_shapes=[dma((6,))],
        compiler_params=pltpu.CompilerParams(vmem_limit_bytes=16 * 2**20),
    )(w_gu0, w_gu1, w_d, out)
    flat = lambda a: a.reshape(2, 2048, 128)
    return flat(gate), flat(up), flat(down), out


def solution(mesh):
    in_specs = (
        P(("gr", "fs"), None),
        P(("gr", "fs")),
        P(None, ("gr", "fs"), "tp"),
        P(None, ("gr", "fs"), "tp"),
        P(None, ("gr", "fs"), "tp"),
        P(("gr", "fs"), None),
        P(("gr", "fs"), None),
    )
    out_specs = (
        P("fs", None, "tp"),
        P("fs", None, "tp"),
        P("fs", None, "tp"),
        P(("gr", "fs"), "tp"),
    )
    return jax.shard_map(
        per_device, mesh=mesh, in_specs=in_specs, out_specs=out_specs, check_vma=False
    )
```

time: 137 us -> 120 us (0.88)
  Pallas kernels: 128 us -> 117 us
  local copies, waits for them, and re-layouts: 8.14 us -> 2.02 us
    pallas_call x1 -> x2, Pallas kernels: 128 us -> 117 us  [the longest x1 115 us: per_device(): pl.pallas_call(kernel, out_shape=(both, both, ready, block), in_specs=[hb...]
    unnamed x12 -> x6, local copies, waits for them, and re-layouts: 8.14 us -> 2.02 us
where the time goes in v2:
time: 120 us
  Pallas kernels  117 us (98%)
  local copies, waits for them, and re-layouts  2.02 us (2%)
    pallas_call x1, Pallas kernels, per_device(): pl.pallas_call(kernel, out_shape=(both, both, ready, block), in_specs=[hb...  115 us

profile of v2, /device:TPU:1, one launch (start us, length us, event | category | flops | bytes accessed | tf_op | source)
XLA Modules:
  0.0 119.8 jit_solution(2483601116480132977)
XLA Ops:
  0.6 0.0 copy-start
  0.6 0.7 copy-done
  1.3 0.0 copy-start.1
  1.3 0.7 copy-done.1
  2.0 0.0 copy-start.2
  2.0 0.7 copy-done.2
  2.7 115.4 %shard_map.102 = (bf16[32,64,256]{2,1,0:T(8,128)(2,1)S(1)}, bf16[32,64,256]{2,1,0:T(8,128)(2,1)S(1)}, bf16[2,32,64,128]{3,2,1,0:T(8,128)(2,1)S(1)}, bf16[512,256]{1,0:T(8,128)(2,1)S(1)}) custom-call(bf16[512,2048]{1,0:T(8,128)(2,1)} %prompt_hbm.1, f32[1,64]{1,0:T(1,128)S(1)} %bitcast.11, f32[16,2,64,128]{3,2,1,0:T(8,128)} %bitcast.12, ...), custom_call_target="tpu_custom_call" | custom-call | tf_op jit(solution)/shard_map/pallas_call | solution.py:457
  118.0 1.8 %shard_map.103 = (bf16[2,32,64,128]{3,2,1,0:T(8,128)(2,1)}, bf16[2,32,64,128]{3,2,1,0:T(8,128)(2,1)}, bf16[2,32,64,128]{3,2,1,0:T(8,128)(2,1)}, bf16[512,256]{1,0:T(8,128)(2,1)}) custom-call(bf16[32,64,256]{2,1,0:T(8,128)(2,1)S(1)} %get-tuple-element.12.w_gu0, bf16[32,64,256]{2,1,0:T(8,128)(2,1)S(1)} %get-tuple-element.13.w_gu1, ...), custom_call_target="tpu_custom_call" | custom-call | tf_op jit(solution)/shard_map/pallas_call | solution.py:505
Async XLA Ops:
  0.6 0.7 copy-start
  1.3 0.7 copy-start.1
  2.0 0.7 copy-start.2

commit v3 on v2

--- a/solution.py
+++ b/solution.py
@@ -12,7 +12,7 @@
 
 PLANES = ((0, 0, 0, 64), (1, 1, 0, 64), (2, -1, 0, 64), (3, 2, 0, 32), (3, -2, 32, 64))
 TOK0, TOK1, HID0, HID1 = 0, 1, 2, 3
-OWN_R, OWN_L, OWN_C, FAR_R, FAR_L, C_L, C_R, C_F0, C_F1 = range(9)
+OWN_R0, OWN_R1, OWN_L0, OWN_L1, OWN_C, FAR_R, FAR_L, C_L, C_R, C_F0, C_F1 = range(11)
 
 
 def kernel(
@@ -26,7 +26,10 @@
     w_gu0,
     w_gu1,
     w_d,
-    blend_v,
+    hi1,
+    lo1,
+    acc,
+    ansb,
     gain_ref,
     routes_ref,
     rw_ref,
@@ -42,9 +45,9 @@
     dx,
     outs,
     ans,
-    s0,
-    s1,
-    acc,
+    ansa,
+    hi0,
+    lo0,
     load_sem,
     wsend,
     wrecv,
@@ -62,34 +65,34 @@
     f = lax.axis_index("fs")
     t = lax.axis_index("tp")
     me = g * 16 + f
-    z = g * 4 + f // 4
-    y = lax.rem(f, 4)
-    x = t // 2
-    c = lax.rem(t, 2)
+    z = g * 4 + (f >> 2)
+    y = f & 3
+    x = t >> 1
+    c = t & 1
 
     def at_zy(zz, yy):
-        zz = lax.rem(zz + 16, 8)
-        yy = lax.rem(yy + 8, 4)
-        return zz // 4, lax.rem(zz, 4) * 4 + yy
-
-    right = (g, f, lax.rem(x + 1, 4) * 2 + c)
-    left = (g, f, lax.rem(x + 3, 4) * 2 + c)
+        zz = (zz + 8) & 7
+        yy = (yy + 4) & 3
+        return zz >> 2, ((zz & 3) << 2) + yy
+
+    right = (g, f, ((x + 1) & 3) * 2 + c)
+    left = (g, f, ((x + 3) & 3) * 2 + c)
     other = (g, f, x * 2 + 1 - c)
-    t_l = lax.rem(x + 3, 4) * 2 + c
-    t_r = lax.rem(x + 1, 4) * 2 + c
-    t_f = lax.rem(x + 2, 4) * 2 + c
+    t_l = ((x + 3) & 3) * 2 + c
+    t_r = ((x + 1) & 3) * 2 + c
+    t_f = ((x + 2) & 3) * 2 + c
 
     barrier = pltpu.get_barrier_semaphore()
 
     def greet_zy(i, carry):
-        gg, ff = at_zy(z + i // 4, y + lax.rem(i, 4))
+        gg, ff = at_zy(z + (i >> 2), y + (i & 3))
         pl.semaphore_signal(barrier, inc=1, device_id=(gg, ff, t), device_id_type=MESH)
         return carry
 
     lax.fori_loop(1, 32, greet_zy, 0)
 
     def greet_tp(i, carry):
-        pl.semaphore_signal(barrier, inc=1, device_id=(g, f, lax.rem(t + i, 8)), device_id_type=MESH)
+        pl.semaphore_signal(barrier, inc=1, device_id=(g, f, (t + i) & 7), device_id_type=MESH)
         return carry
 
     lax.fori_loop(1, 8, greet_tp, 0)
@@ -125,7 +128,7 @@
 
     def send_w(stage, dest, sem, rows):
         def body(i, carry):
-            gg, ff = at_zy(z + i // 4, y + lax.rem(i, 4))
+            gg, ff = at_zy(z + (i >> 2), y + (i & 3))
             pltpu.make_async_remote_copy(
                 src_ref=stage.at[ff, rows],
                 dst_ref=dest.at[me, rows],
@@ -161,17 +164,22 @@
         return ref if half is None else ref.at[pl.ds(512 * half, 512)]
 
     def ag_own(kind):
-        ref = piece(kind, t, None)
-        copy_to(ref, kind, OWN_R, right).start()
-        copy_to(ref, kind, OWN_L, left).start()
-        copy_to(ref, kind, OWN_C, other).start()
+        copy_to(piece(kind, t, 0), kind, OWN_R0, right).start()
+        copy_to(piece(kind, t, 1), kind, OWN_L1, left).start()
+        copy_to(piece(kind, t, 1), kind, OWN_R1, right).start()
+        copy_to(piece(kind, t, 0), kind, OWN_L0, left).start()
+        copy_to(piece(kind, t, None), kind, OWN_C, other).start()
 
     def ag_relay(kind):
-        copy_to(piece(kind, t_l, None), kind, OWN_R, right).wait_recv()
+        copy_to(piece(kind, t_l, 0), kind, OWN_R0, right).wait_recv()
         copy_to(piece(kind, t_l, 0), kind, FAR_R, right).start()
+        copy_to(piece(kind, t_r, 1), kind, OWN_L1, left).wait_recv()
+        copy_to(piece(kind, t_r, 1), kind, FAR_L, left).start()
+
+    def ag_pass(kind):
+        copy_to(piece(kind, t_l, 1), kind, OWN_R1, right).wait_recv()
         copy_to(piece(kind, t_l, None), kind, C_L, other).start()
-        copy_to(piece(kind, t_r, None), kind, OWN_L, left).wait_recv()
-        copy_to(piece(kind, t_r, 1), kind, FAR_L, left).start()
+        copy_to(piece(kind, t_r, 0), kind, OWN_L0, left).wait_recv()
         copy_to(piece(kind, t_r, None), kind, C_R, other).start()
 
     def ag_far(kind):
@@ -185,18 +193,10 @@
             copy_to(piece(kind, t, half), kind, i, other).wait_recv()
 
     def ag_drain(kind):
-        for i, half in (
-            (OWN_R, None),
-            (OWN_L, None),
-            (OWN_C, None),
-            (FAR_R, 0),
-            (FAR_L, 1),
-            (C_L, None),
-            (C_R, None),
-            (C_F0, 0),
-            (C_F1, 1),
-        ):
-            copy_to(piece(kind, t, half), kind, i, other).wait_send()
+        for i in (OWN_C, C_L, C_R):
+            copy_to(piece(kind, t, None), kind, i, other).wait_send()
+        for i in (OWN_R0, OWN_R1, OWN_L0, OWN_L1, FAR_R, FAR_L, C_F0, C_F1):
+            copy_to(piece(kind, t, 0), kind, i, other).wait_send()
 
     def send_tokens(p):
         for j, dz, lo, hi in PLANES:
@@ -218,6 +218,9 @@
         part = slots_x.at[p, pl.ds(0, 15)]
         pltpu.make_async_copy(part, part, sems.at[p]).wait()
 
+    def back(p, sem):
+        return (ans, ansa, ansb)[sem]
+
     def send_back(p, plane, sem, lanes):
         for j, dz, lo, hi in PLANES:
             for dy in range(4):
@@ -225,15 +228,15 @@
                     continue
                 gg, ff = at_zy(z - dz, y + dy)
                 pltpu.make_async_remote_copy(
-                    src_ref=outs.at[p, j * 4 + lax.rem(y + dy, 4), pl.ds(lo, hi - lo), lanes],
-                    dst_ref=ans.at[p, f, pl.ds(lo, hi - lo), lanes],
+                    src_ref=outs.at[p, j * 4 + ((y + dy) & 3), pl.ds(lo, hi - lo), lanes],
+                    dst_ref=back(p, sem).at[f, pl.ds(lo, hi - lo)],
                     send_sem=rsend.at[sem],
                     recv_sem=rrecv.at[sem],
                     device_id=(gg, ff, t),
                     device_id_type=MESH,
                 ).start()
         if plane == 0:
-            ans[p, f, :, lanes] = outs[p, y, :, lanes]
+            back(p, sem)[f] = outs[p, y, :, lanes]
 
     def await_back(sems, p, sem, lanes):
         part = outs.at[p, pl.ds(0, 15), :, lanes]
@@ -241,7 +244,7 @@
 
     def send_dx(p, h):
         def body(i, carry):
-            tt = lax.rem(t + i, 8)
+            tt = (t + i) & 7
             pltpu.make_async_remote_copy(
                 src_ref=w_d.at[p, pl.ds(tt * 4, 4), pl.ds(32 * h, 32)],
                 dst_ref=dx.at[p, h, t],
@@ -287,25 +290,16 @@
             outs[p, pl.ds(r * 4, 4), :, lanes] = value.reshape(4, 64, 128 * len(halves))
             send_back(p, r, sem, lanes)
 
-    def blend(p, lanes):
+    def blend(p, sem, lanes):
         for r in range(2):
             rows = pl.ds(r * 256, 256)
-            here = slice(r * 256, r * 256 + 256)
-            values = ans[p, :, :, lanes].reshape(1024, lanes.size)
-            first = jnp.dot(s0[p, rows], values, preferred_element_type=F32)
-            second = jnp.dot(s1[p, rows], values, preferred_element_type=F32)
-            part = rw0[here] * first + rw1[here] * second
+            values = back(p, sem)[...].reshape(1024, lanes.size)
+            part = jnp.dot((hi0, hi1)[p][rows], values, preferred_element_type=F32)
+            part += jnp.dot((lo0, lo1)[p][rows], values, preferred_element_type=F32)
             if p == 0:
                 acc[rows] = part
             else:
                 acc[rows, lanes] += part
-
-    def place_columns():
-        a = lax.broadcasted_iota(jnp.int32, (256, 256), 0)
-        b = lax.broadcasted_iota(jnp.int32, (256, 256), 1)
-        goes = a == ((b >> 5) & 1) * 128 + (b >> 6) * 32 + (b & 31)
-        to_place = jnp.where(goes, 1.0, 0.0).astype(BF)
-        blend_v[...] = jnp.dot(acc[...].astype(BF), to_place, preferred_element_type=F32).astype(BF)
 
     whole = pl.ds(0, 256)
     low, high = pl.ds(0, 128), pl.ds(128, 128)
@@ -350,7 +344,6 @@
     pl.semaphore_wait(barrier, 38)
     send_tokens(0)
     send_tokens(1)
-    send_w(stage_d.at[0], w_d.at[0], 0, all_rows)
     loads[2].wait()
     loads[3].wait()
     loads[5].wait()
@@ -360,50 +353,57 @@
     send_w(stage_gu.at[0], w_gu0, 2, all_rows)
     round_gu(1, gain)
     send_w(stage_gu.at[1], w_gu1, 3, all_rows)
+    send_w(stage_d.at[0], w_d.at[0], 0, all_rows)
     round_d(1)
     send_w(stage_d.at[1], w_d.at[1], 1, rows_a)
+    send_w(stage_d.at[1], w_d.at[1], 4, rows_b)
     await_tokens(trecv, 0)
     ag_own(TOK0)
     await_tokens(trecv, 1)
     ag_own(TOK1)
+    loads[6].wait()
     slot0 = column(slot0_row)
     slot1 = column(slot1_row)
-    for p in range(2):
-        number = (lax.broadcasted_iota(jnp.int32, (512, 1024), 1) + p * 1024).astype(F32)
-        s0[p] = jnp.where(number == slot0, 1.0, 0.0).astype(BF)
-        s1[p] = jnp.where(number == slot1, 1.0, 0.0).astype(BF)
-    loads[6].wait()
     rw0 = column(rw_ref[0:1])
     rw1 = column(rw_ref[1:2])
+    for p in range(2):
+        for r in range(4):
+            cols = pl.ds(r * 256, 256)
+            number = (lax.broadcasted_iota(jnp.int32, (512, 256), 1) + (p * 1024 + r * 256)).astype(F32)
+            weight = jnp.where(number == slot0, rw0, jnp.where(number == slot1, rw1, 0.0))
+            upper = weight.astype(BF)
+            (hi0, hi1)[p][:, cols] = upper
+            (lo0, lo1)[p][:, cols] = (weight - upper.astype(F32)).astype(BF)
     ag_relay(TOK0)
+    ag_pass(TOK0)
     ag_relay(TOK1)
     ag_far(TOK0)
+    ag_pass(TOK1)
     ag_far(TOK1)
     ag_end(TOK0)
-    ag_end(TOK1)
-    await_w(wrecv, w_d.at[0], 0, all_rows)
-    send_dx(0, 0)
-    send_dx(0, 1)
     await_w(wrecv, w_gu0, 2, all_rows)
     hidden(0)
     ag_own(HID0)
+    ag_end(TOK1)
     ag_relay(HID0)
+    ag_pass(HID0)
     ag_far(HID0)
-    await_dx(drecv, 0, 0)
-    await_dx(drecv, 0, 1)
     ag_end(HID0)
-    expert_out(0, (0, 1), 0, whole)
-    send_w(stage_d.at[1], w_d.at[1], 4, rows_b)
     await_w(wrecv, w_gu1, 3, all_rows)
     hidden(1)
     ag_own(HID1)
     ag_relay(HID1)
+    ag_pass(HID1)
+    await_w(wrecv, w_d.at[0], 0, all_rows)
+    send_dx(0, 0)
+    send_dx(0, 1)
     ag_far(HID1)
+    ag_end(HID1)
+    await_dx(drecv, 0, 0)
+    await_dx(drecv, 0, 1)
+    expert_out(0, (0, 1), 0, whole)
     await_w(wrecv, w_d.at[1], 1, rows_a)
     send_dx(1, 0)
-    ag_end(HID1)
-    await_back(rrecv, 0, 0, whole)
-    blend(0, whole)
     await_w(wrecv, w_d.at[1], 4, rows_b)
     send_dx(1, 1)
     await_dx(drecv, 1, 0)
@@ -421,17 +421,31 @@
     await_w(wsend, w_gu0, 2, all_rows)
     await_w(wsend, w_gu1, 3, all_rows)
     await_w(wsend, w_d.at[1], 4, rows_b)
+    await_back(rrecv, 0, 0, whole)
+    blend(0, 0, whole)
     await_back(rsend, 0, 0, whole)
     await_back(rrecv, 1, 1, low)
-    blend(1, low)
-    await_back(rrecv, 1, 2, high)
-    blend(1, high)
-    place_columns()
+    blend(1, 1, low)
     await_back(rsend, 1, 1, low)
     await_back(rsend, 1, 2, high)
-
-
-def copy_out(w_gu0, w_gu1, w_d, blend_v, gate_out, up_out, down_out, blend_out, sem):
+    await_back(rrecv, 1, 2, high)
+
+
+def copy_out(
+    w_gu0,
+    w_gu1,
+    w_d,
+    hi1,
+    lo1,
+    acc,
+    ansb,
+    gate_out,
+    up_out,
+    down_out,
+    blend_out,
+    blend_v,
+    sem,
+):
     copies = [
         pltpu.make_async_copy(w_gu0.at[:, :, pl.ds(0, 128)], gate_out.at[0], sem.at[0]),
         pltpu.make_async_copy(w_gu1.at[:, :, pl.ds(0, 128)], gate_out.at[1], sem.at[1]),
@@ -440,8 +454,18 @@
         pltpu.make_async_copy(w_d, down_out, sem.at[4]),
         pltpu.make_async_copy(blend_v, blend_out, sem.at[5]),
     ]
-    for cp in copies:
+    for cp in copies[:5]:
         cp.start()
+    a = lax.broadcasted_iota(jnp.int32, (256, 256), 0)
+    b = lax.broadcasted_iota(jnp.int32, (256, 256), 1)
+    goes = a == ((b >> 5) & 1) * 128 + (b >> 6) * 32 + (b & 31)
+    to_place = jnp.where(goes, 1.0, 0.0).astype(BF)
+    values = ansb[...].reshape(1024, 128)
+    part = jnp.dot(hi1[...], values, preferred_element_type=F32)
+    part += jnp.dot(lo1[...], values, preferred_element_type=F32)
+    total = jnp.concatenate([acc[:, 0:128], acc[:, 128:256] + part], axis=1).astype(BF)
+    blend_v[...] = jnp.dot(total, to_place, preferred_element_type=F32).astype(BF)
+    copies[5].start()
     for cp in copies:
         cp.wait()
 
@@ -452,13 +476,16 @@
     ready = jax.ShapeDtypeStruct((2, 32, 64, 128), BF)
     both = jax.ShapeDtypeStruct((32, 64, 256), BF)
     block = jax.ShapeDtypeStruct((512, 256), BF)
+    select = jax.ShapeDtypeStruct((512, 1024), BF)
+    total = jax.ShapeDtypeStruct((512, 256), F32)
+    part = jax.ShapeDtypeStruct((16, 64, 128), BF)
     dma = pltpu.SemaphoreType.DMA
     split = lambda a: a.reshape(16, 2, 64, 128)
-    w_gu0, w_gu1, w_d, out = pl.pallas_call(
+    passed = pl.pallas_call(
         kernel,
-        out_shape=(both, both, ready, block),
+        out_shape=(both, both, ready, select, select, total, part),
         in_specs=[hbm] * 7,
-        out_specs=(vmem,) * 4,
+        out_specs=(vmem,) * 7,
         scratch_shapes=[
             pltpu.VMEM((1, 64), F32),
             pltpu.VMEM((2, 512), jnp.int32),
@@ -474,24 +501,24 @@
             pltpu.VMEM((2, 8, 1024, 128), BF),
             pltpu.VMEM((2, 2, 8, 4, 32, 128), BF),
             pltpu.VMEM((2, 16, 64, 256), BF),
-            pltpu.VMEM((2, 16, 64, 256), BF),
-            pltpu.VMEM((2, 512, 1024), BF),
-            pltpu.VMEM((2, 512, 1024), BF),
-            pltpu.VMEM((512, 256), F32),
+            pltpu.VMEM((16, 64, 256), BF),
+            pltpu.VMEM((16, 64, 128), BF),
+            pltpu.VMEM((512, 1024), BF),
+            pltpu.VMEM((512, 1024), BF),
             dma((7,)),
             dma((5,)),
             dma((5,)),
             dma((2,)),
             dma((2,)),
-            dma((4, 9)),
-            dma((4, 9)),
+            dma((4, 11)),
+            dma((4, 11)),
             dma((2, 2)),
             dma((2, 2)),
             dma((3,)),
             dma((3,)),
         ],
         compiler_params=pltpu.CompilerParams(
-            collective_id=0, has_side_effects=True, vmem_limit_bytes=50 * 2**20
+            collective_id=0, has_side_effects=True, vmem_limit_bytes=48 * 2**20
         ),
     )(
         prompt,
@@ -505,11 +532,11 @@
     gate, up, down, out = pl.pallas_call(
         copy_out,
         out_shape=(ready, ready, ready, block),
-        in_specs=[vmem] * 4,
+        in_specs=[vmem] * 7,
         out_specs=(hbm,) * 4,
-        scratch_shapes=[dma((6,))],
+        scratch_shapes=[pltpu.VMEM((512, 256), BF), dma((6,))],
         compiler_params=pltpu.CompilerParams(vmem_limit_bytes=16 * 2**20),
-    )(w_gu0, w_gu1, w_d, out)
+    )(*passed)
     flat = lambda a: a.reshape(2, 2048, 128)
     return flat(gate), flat(up), flat(down), out
 

time: 120 us -> 114 us (0.950)
  Pallas kernels: 117 us -> 112 us
    pallas_call x1, Pallas kernels: 115 us -> 109 us  [per_device(): pl.pallas_call(kernel, out_shape=(both, both, ready, select, select, tota...]
where the time goes in v3:
time: 114 us
  Pallas kernels  112 us (98%)
  local copies, waits for them, and re-layouts  2.02 us (2%)
    pallas_call x1, Pallas kernels, per_device(): pl.pallas_call(kernel, out_shape=(both, both, ready, select, select, tota...  109 us
    pallas_call x1, Pallas kernels, per_device(): pl.pallas_call(copy_out, out_shape=(ready, ready, ready, block), in_specs...  2.45 us

profile of v3, /device:TPU:1, one launch (start us, length us, event | category | flops | bytes accessed | tf_op | source)
XLA Modules:
  0.0 114.3 jit_solution(17609661900938480558)
XLA Ops:
  0.6 0.0 copy-start
  0.6 0.7 copy-done
  1.3 0.0 copy-start.1
  1.3 0.7 copy-done.1
  2.0 0.0 copy-start.2
  2.0 0.7 copy-done.2
  2.7 109.1 %shard_map.102 = (bf16[32,64,256]{2,1,0:T(8,128)(2,1)S(1)}, bf16[32,64,256]{2,1,0:T(8,128)(2,1)S(1)}, bf16[2,32,64,128]{3,2,1,0:T(8,128)(2,1)S(1)}, bf16[512,102...) custom-call(bf16[512,2048]{1,0:T(8,128)(2,1)} %prompt_hbm.1, ...), custom_call_target="tpu_custom_call" | custom-call | tf_op jit(solution)/shard_map/pallas_call | solution.py:484
  111.8 2.5 %shard_map.103 = (bf16[2,32,64,128]{3,2,1,0:T(8,128)(2,1)}, bf16[2,32,64,128]{3,2,1,0:T(8,128)(2,1)}, bf16[2,32,64,128]{3,2,1,0:T(8,128)(2,1)}, bf16[512,256]{1,0:T(8,128)(2,1)}) custom-call(bf16[32,64,256]{2,1,0:T(8,128)(2,1)S(1)} %get-tuple-element.15.w_gu0, bf16[32,64,256]{2,1,0:T(8,128)(2,1)S(1)} %get-tuple-element.16.w_gu1, ...), custom_call_target="tpu_custom_call" | custom-call | tf_op jit(solution)/shard_map/pallas_call | solution.py:532
Async XLA Ops:
  0.6 0.7 copy-start
  1.3 0.7 copy-start.1
  2.0 0.7 copy-start.2

commit v4 on v3

--- a/solution.py
+++ b/solution.py
@@ -400,10 +400,10 @@
     ag_far(HID1)
     ag_end(HID1)
     await_dx(drecv, 0, 0)
+    await_w(wrecv, w_d.at[1], 1, rows_a)
+    send_dx(1, 0)
     await_dx(drecv, 0, 1)
     expert_out(0, (0, 1), 0, whole)
-    await_w(wrecv, w_d.at[1], 1, rows_a)
-    send_dx(1, 0)
     await_w(wrecv, w_d.at[1], 4, rows_b)
     send_dx(1, 1)
     await_dx(drecv, 1, 0)
@@ -521,13 +521,18 @@
             collective_id=0, has_side_effects=True, vmem_limit_bytes=48 * 2**20
         ),
     )(
-        prompt,
-        norm_gain.reshape(1, 64),
-        split(gate_master),
-        split(up_master),
-        split(down_master),
-        routes.T,
-        route_weights.T,
+        *[
+            pltpu.with_memory_space_constraint(a, pltpu.HBM)
+            for a in (
+                prompt,
+                norm_gain.reshape(1, 64),
+                split(gate_master),
+                split(up_master),
+                split(down_master),
+                routes.T,
+                route_weights.T,
+            )
+        ]
     )
     gate, up, down, out = pl.pallas_call(
         copy_out,

time: 114 us -> 111 us (0.974)
  local copies, waits for them, and re-layouts: 2.02 us -> 0 us
    unnamed x6 -> x0, local copies, waits for them, and re-layouts: 2.02 us -> none
where the time goes in v4:
time: 111 us
  Pallas kernels  111 us (100%)
    pallas_call x1, Pallas kernels, per_device(): pl.pallas_call(kernel, out_shape=(both, both, ready, select, select, tota...  108 us
    pallas_call x1, Pallas kernels, per_device(): pl.pallas_call(copy_out, out_shape=(ready, ready, ready, block), in_specs...  2.45 us

profile of v4, /device:TPU:1, one launch (start us, length us, event | category | flops | bytes accessed | tf_op | source)
XLA Modules:
  0.0 111.3 jit_solution(14235332200450068087)
XLA Ops:
  0.6 108.2 %shard_map.102 = (bf16[32,64,256]{2,1,0:T(8,128)(2,1)S(1)}, bf16[32,64,256]{2,1,0:T(8,128)(2,1)S(1)}, bf16[2,32,64,128]{3,2,1,0:T(8,128)(2,1)S(1)}, bf16[512,102...) custom-call(bf16[512,2048]{1,0:T(8,128)(2,1)} %prompt_hbm.1, ...), custom_call_target="tpu_custom_call" | custom-call | tf_op jit(solution)/shard_map/pallas_call | solution.py:484
  108.8 2.4 %shard_map.103 = (bf16[2,32,64,128]{3,2,1,0:T(8,128)(2,1)}, bf16[2,32,64,128]{3,2,1,0:T(8,128)(2,1)}, bf16[2,32,64,128]{3,2,1,0:T(8,128)(2,1)}, bf16[512,256]{1,0:T(8,128)(2,1)}) custom-call(bf16[32,64,256]{2,1,0:T(8,128)(2,1)S(1)} %get-tuple-element.15.w_gu0, bf16[32,64,256]{2,1,0:T(8,128)(2,1)S(1)} %get-tuple-element.16.w_gu1, ...), custom_call_target="tpu_custom_call" | custom-call | tf_op jit(solution)/shard_map/pallas_call | solution.py:537

commit v5 on v4

--- a/solution.py
+++ b/solution.py
@@ -40,6 +40,11 @@
     stage_gu,
     stage_d,
     slots_x,
+    near_x,
+    near_m,
+    got_x,
+    got_m,
+    spread,
     tok,
     hid,
     dx,
@@ -53,6 +58,8 @@
     wrecv,
     tsend,
     trecv,
+    nsend,
+    nrecv,
     asend,
     arecv,
     dsend,
@@ -126,8 +133,9 @@
         lax.fori_loop(0, 16, body, 0)
         w_gu[p][me] = stage_gu[p, f]
 
-    def send_w(stage, dest, sem, rows):
-        def body(i, carry):
+    def send_w(stage, dest, sem, rows, first=1, last=32, step=1):
+        def body(n, carry):
+            i = n * step
             gg, ff = at_zy(z + (i >> 2), y + (i & 3))
             pltpu.make_async_remote_copy(
                 src_ref=stage.at[ff, rows],
@@ -139,7 +147,23 @@
             ).start()
             return carry
 
-        lax.fori_loop(1, 32, body, 0)
+        lax.fori_loop(first, last, body, 0)
+
+    def send_w_other(stage, dest, sem):
+        def body(n, carry):
+            i = n + n // 3 + 1
+            gg, ff = at_zy(z + (i >> 2), y + (i & 3))
+            pltpu.make_async_remote_copy(
+                src_ref=stage.at[ff],
+                dst_ref=dest.at[me],
+                send_sem=wsend.at[sem],
+                recv_sem=wrecv.at[sem],
+                device_id=(gg, ff, t),
+                device_id_type=MESH,
+            ).start()
+            return carry
+
+        lax.fori_loop(0, 24, body, 0)
 
     def await_w(sems, dest, sem, rows):
         part = dest.at[pl.ds(0, 31), rows]
@@ -201,21 +225,55 @@
     def send_tokens(p):
         for j, dz, lo, hi in PLANES:
             for dy in range(4):
+                if j in (1, 2) or (dz == 0 and dy == 0):
+                    continue
                 gg, ff = at_zy(z + dz, y + dy)
-                if dz == 0 and dy == 0:
-                    continue
                 pltpu.make_async_remote_copy(
-                    src_ref=slots_x.at[p, ff, pl.ds(lo, hi - lo)],
+                    src_ref=slots_x.at[p, j // 3, (y + dy) & 3, pl.ds(lo, hi - lo)],
                     dst_ref=tok.at[p, t, j * 4 + y, pl.ds(lo, hi - lo)],
                     send_sem=tsend.at[p],
                     recv_sem=trecv.at[p],
                     device_id=(gg, ff, t),
                     device_id_type=MESH,
                 ).start()
-        tok[p, t, y] = slots_x[p, f]
+        tok[p, t, y] = slots_x[p, 0, y]
+
+    def near_copies(d):
+        gg, ff = at_zy(z + 1 - 2 * d, y)
+        return [
+            pltpu.make_async_remote_copy(
+                src_ref=src.at[d],
+                dst_ref=dst.at[d],
+                send_sem=nsend.at[d, i],
+                recv_sem=nrecv.at[d, i],
+                device_id=(gg, ff, t),
+                device_id_type=MESH,
+            )
+            for i, (src, dst) in enumerate(((near_x, got_x), (near_m, got_m)))
+        ]
+
+    def pass_near(d):
+        for cp in near_copies(d):
+            cp.wait_recv()
+        for p in range(2):
+            number = (lax.broadcasted_iota(jnp.int32, (256, 256), 0) + p * 256).astype(F32)
+            pick = (number == got_m[d, 0:1]) | (number == got_m[d, 1:2])
+            rows = jnp.dot(jnp.where(pick, 1.0, 0.0).astype(BF), got_x[d], preferred_element_type=F32)
+            spread[d, p] = rows.astype(BF).reshape(4, 64, 256)
+            for dy in (2, 1, 3):
+                gg, ff = at_zy(z, y + dy)
+                pltpu.make_async_remote_copy(
+                    src_ref=spread.at[d, p, (y + dy) & 3],
+                    dst_ref=tok.at[p, t, (d + 1) * 4 + y],
+                    send_sem=tsend.at[p],
+                    recv_sem=trecv.at[p],
+                    device_id=(gg, ff, t),
+                    device_id_type=MESH,
+                ).start()
+            tok[p, t, (d + 1) * 4 + y] = spread[d, p, y]
 
     def await_tokens(sems, p):
-        part = slots_x.at[p, pl.ds(0, 15)]
+        part = tok.at[p, t, pl.ds(0, 13)]
         pltpu.make_async_copy(part, part, sems.at[p]).wait()
 
     def back(p, sem):
@@ -330,18 +388,52 @@
     mine = prompt_v[:, pl.ds(pl.multiple_of(t * 256, 256), 256)].astype(F32)
     normed = (mine * scale).astype(BF)
 
+    def group_of(dz):
+        return ((z + dz) & 3).astype(F32)
+
+    numbers = lax.broadcasted_iota(jnp.int32, (256, 512), 0).astype(F32)
+
     def pick_slots(p):
-        for r in range(4):
-            number = (lax.broadcasted_iota(jnp.int32, (256, 512), 0) + (p * 1024 + r * 256)).astype(F32)
+        for j in range(2):
+            number = numbers + (group_of(2 * j) * 256.0 + p * 1024.0)
             pick = jnp.where((number == slot0_row) | (number == slot1_row), 1.0, 0.0).astype(BF)
             rows = jnp.dot(pick, normed, preferred_element_type=F32).astype(BF)
-            slots_x[p, pl.ds(r * 4, 4)] = rows.reshape(4, 64, 256)
-
+            slots_x[p, j] = rows.reshape(4, 64, 256)
+
+    def along(values, hit):
+        return jnp.sum(values.astype(F32) * hit, axis=0, keepdims=True)
+
+    group_row = along(experts >> 3, hit0)
+    groups = lax.broadcasted_iota(jnp.int32, (8, 512), 0).astype(F32)
+    group_hit = jnp.where(groups == group_row, 1.0, 0.0)
+    group_rank = jnp.dot(group_hit.astype(BF), before, preferred_element_type=F32)
+    number_row = along(group_rank, group_hit) + group_row * 256.0
+    facts = (
+        along(experts & 1, hit0),
+        along((experts >> 1) & 3, hit0),
+        along(rank0, hit0),
+        along(experts & 1, hit1),
+        along((experts >> 1) & 3, hit1),
+        along(rank1, hit1),
+        jnp.ones((1, 512), F32),
+        jnp.zeros((1, 512), F32),
+    )
+    facts = jnp.concatenate(facts, axis=0).astype(BF)
+    for d in range(2):
+        pick = jnp.where(numbers + group_of(1 - 2 * d) * 256.0 == number_row, 1.0, 0.0).astype(BF)
+        near_x[d] = jnp.dot(pick, normed, preferred_element_type=F32).astype(BF)
+        m = lax.dot_general(facts, pick, (((1,), (1,)), ((), ())), preferred_element_type=F32)
+        first = m[0:1] * 256.0 + m[1:2] * 64.0 + m[2:3] + (m[6:7] - 1.0)
+        second = m[3:4] * 256.0 + m[4:5] * 64.0 + m[5:6] + (m[6:7] - 1.0)
+        near_m[d] = jnp.concatenate([first, second, m[2:8]], axis=0)
     pick_slots(0)
     pick_slots(1)
     loads[4].wait()
     round_d(0)
     pl.semaphore_wait(barrier, 38)
+    for d in range(2):
+        for cp in near_copies(d):
+            cp.start()
     send_tokens(0)
     send_tokens(1)
     loads[2].wait()
@@ -350,8 +442,11 @@
     eye = lax.broadcasted_iota(jnp.int32, (64, 64), 0) == lax.broadcasted_iota(jnp.int32, (64, 64), 1)
     gain = jnp.sum(jnp.where(eye, gain_ref[...], 0.0), axis=1, keepdims=True)
     round_gu(0, gain)
-    send_w(stage_gu.at[0], w_gu0, 2, all_rows)
+    send_w(stage_gu.at[0], w_gu0, 2, all_rows, 1, 8, 4)
     round_gu(1, gain)
+    pass_near(0)
+    pass_near(1)
+    send_w_other(stage_gu.at[0], w_gu0, 2)
     send_w(stage_gu.at[1], w_gu1, 3, all_rows)
     send_w(stage_d.at[0], w_d.at[0], 0, all_rows)
     round_d(1)
@@ -412,6 +507,9 @@
     expert_out(1, (1,), 2, high)
     for kind in range(4):
         ag_drain(kind)
+    for d in range(2):
+        for cp in near_copies(d):
+            cp.wait_send()
     for p in range(2):
         await_tokens(tsend, p)
         for h in range(2):
@@ -496,7 +594,12 @@
             pltpu.VMEM((16, 2, 64, 128), F32),
             pltpu.VMEM((2, 16, 64, 256), BF),
             pltpu.VMEM((2, 16, 64, 128), BF),
-            pltpu.VMEM((2, 16, 64, 256), BF),
+            pltpu.VMEM((2, 2, 4, 64, 256), BF),
+            pltpu.VMEM((2, 256, 256), BF),
+            pltpu.VMEM((2, 8, 256), F32),
+            pltpu.VMEM((2, 256, 256), BF),
+            pltpu.VMEM((2, 8, 256), F32),
+            pltpu.VMEM((2, 2, 4, 64, 256), BF),
             pltpu.VMEM((2, 8, 16, 64, 256), BF),
             pltpu.VMEM((2, 8, 1024, 128), BF),
             pltpu.VMEM((2, 2, 8, 4, 32, 128), BF),
@@ -510,6 +613,8 @@
             dma((5,)),
             dma((2,)),
             dma((2,)),
+            dma((2, 2)),
+            dma((2, 2)),
             dma((4, 11)),
             dma((4, 11)),
             dma((2, 2)),

time: 111 us -> 110 us (level)
  Pallas kernels: 111 us -> 109 us
    pallas_call x1, Pallas kernels: 108 us -> 107 us  [per_device(): pl.pallas_call(kernel, out_shape=(both, both, ready, select, select, tota...]
where the time goes in v5:
time: 110 us
  Pallas kernels  109 us (99%)
    pallas_call x1, Pallas kernels, per_device(): pl.pallas_call(kernel, out_shape=(both, both, ready, select, select, tota...  107 us
    pallas_call x1, Pallas kernels, per_device(): pl.pallas_call(copy_out, out_shape=(ready, ready, ready, block), in_specs...  2.45 us

profile of v5, /device:TPU:1, one launch (start us, length us, event | category | flops | bytes accessed | tf_op | source)
XLA Modules:
  0.0 109.8 jit_solution(7076355582197098427)
XLA Ops:
  0.6 106.7 %shard_map.102 = (bf16[32,64,256]{2,1,0:T(8,128)(2,1)S(1)}, bf16[32,64,256]{2,1,0:T(8,128)(2,1)S(1)}, bf16[2,32,64,128]{3,2,1,0:T(8,128)(2,1)S(1)}, bf16[512,102...) custom-call(bf16[512,2048]{1,0:T(8,128)(2,1)} %prompt_hbm.1, ...), custom_call_target="tpu_custom_call" | custom-call | tf_op jit(solution)/shard_map/pallas_call | solution.py:582
  107.4 2.4 %shard_map.103 = (bf16[2,32,64,128]{3,2,1,0:T(8,128)(2,1)}, bf16[2,32,64,128]{3,2,1,0:T(8,128)(2,1)}, bf16[2,32,64,128]{3,2,1,0:T(8,128)(2,1)}, bf16[512,256]{1,0:T(8,128)(2,1)}) custom-call(bf16[32,64,256]{2,1,0:T(8,128)(2,1)S(1)} %get-tuple-element.15.w_gu0, bf16[32,64,256]{2,1,0:T(8,128)(2,1)S(1)} %get-tuple-element.16.w_gu1, ...), custom_call_target="tpu_custom_call" | custom-call | tf_op jit(solution)/shard_map/pallas_call | solution.py:642

commit v6 on v5

--- a/solution.py
+++ b/solution.py
@@ -10,9 +10,11 @@
 BF = jnp.bfloat16
 F32 = jnp.float32
 
-PLANES = ((0, 0, 0, 64), (1, 1, 0, 64), (2, -1, 0, 64), (3, 2, 0, 32), (3, -2, 32, 64))
+PLANES = ((0, 0, 0, 64), (1, 2, 0, 32), (1, -2, 32, 64), (2, 1, 0, 64), (3, -1, 0, 64))
 TOK0, TOK1, HID0, HID1 = 0, 1, 2, 3
-OWN_R0, OWN_R1, OWN_L0, OWN_L1, OWN_C, FAR_R, FAR_L, C_L, C_R, C_F0, C_F1 = range(11)
+TO_R, TO_L, TO_L2, FAR_R, FAR_L, ACROSS = 0, 3, 4, 5, 6, 7
+PIECES = ((0, 4), (4, 4), (8, 8), (0, 8), (0, 16))
+FIRST, WHOLE = 3, 4
 
 
 def kernel(
@@ -173,66 +175,69 @@
         return pltpu.make_async_remote_copy(
             src_ref=ref,
             dst_ref=ref,
-            send_sem=asend.at[sems, i],
+            send_sem=asend.at[sems],
             recv_sem=arecv.at[sems, i],
             device_id=where,
             device_id_type=MESH,
         )
 
-    def piece(kind, tt, half):
-        p = kind % 2
+    def piece(kind, tt, part):
+        lo, size = PIECES[part]
         if kind < 2:
-            ref = tok.at[p, tt]
-            return ref if half is None else ref.at[pl.ds(8 * half, 8)]
-        ref = hid.at[p, tt]
-        return ref if half is None else ref.at[pl.ds(512 * half, 512)]
-
-    def ag_own(kind):
-        copy_to(piece(kind, t, 0), kind, OWN_R0, right).start()
-        copy_to(piece(kind, t, 1), kind, OWN_L1, left).start()
-        copy_to(piece(kind, t, 1), kind, OWN_R1, right).start()
-        copy_to(piece(kind, t, 0), kind, OWN_L0, left).start()
-        copy_to(piece(kind, t, None), kind, OWN_C, other).start()
-
-    def ag_relay(kind):
-        copy_to(piece(kind, t_l, 0), kind, OWN_R0, right).wait_recv()
-        copy_to(piece(kind, t_l, 0), kind, FAR_R, right).start()
-        copy_to(piece(kind, t_r, 1), kind, OWN_L1, left).wait_recv()
-        copy_to(piece(kind, t_r, 1), kind, FAR_L, left).start()
+            return tok.at[kind, tt, pl.ds(lo, size)]
+        return hid.at[kind - 2, tt, pl.ds(64 * lo, 64 * size)]
+
+    def own_right(kind, part):
+        copy_to(piece(kind, t, part), kind, TO_R + part, right).start()
+
+    def own_left(kind, part):
+        copy_to(piece(kind, t, part), kind, TO_L2 if part == 2 else TO_L, left).start()
+
+    def own_other(kind):
+        copy_to(piece(kind, t, WHOLE), kind, ACROSS, other).start()
+
+    def relay_right(kind, part):
+        copy_to(piece(kind, t_l, part), kind, TO_R + part, right).wait_recv()
+        copy_to(piece(kind, t_l, part), kind, FAR_R, right).start()
+
+    def relay_left(kind):
+        copy_to(piece(kind, t_r, 2), kind, TO_L2, left).wait_recv()
+        copy_to(piece(kind, t_r, 2), kind, FAR_L, left).start()
 
     def ag_pass(kind):
-        copy_to(piece(kind, t_l, 1), kind, OWN_R1, right).wait_recv()
-        copy_to(piece(kind, t_l, None), kind, C_L, other).start()
-        copy_to(piece(kind, t_r, 0), kind, OWN_L0, left).wait_recv()
-        copy_to(piece(kind, t_r, None), kind, C_R, other).start()
+        copy_to(piece(kind, t_l, 2), kind, TO_R + 2, right).wait_recv()
+        copy_to(piece(kind, t_l, WHOLE), kind, ACROSS, other).start()
+        copy_to(piece(kind, t_r, FIRST), kind, TO_L, left).wait_recv()
+        copy_to(piece(kind, t_r, WHOLE), kind, ACROSS, other).start()
 
     def ag_far(kind):
-        copy_to(piece(kind, t_f, 0), kind, FAR_R, right).wait_recv()
-        copy_to(piece(kind, t_f, 0), kind, C_F0, other).start()
-        copy_to(piece(kind, t_f, 1), kind, FAR_L, left).wait_recv()
-        copy_to(piece(kind, t_f, 1), kind, C_F1, other).start()
+        copy_to(piece(kind, t_f, FIRST), kind, FAR_R, right).wait_recv()
+        copy_to(piece(kind, t_f, FIRST), kind, ACROSS, other).start()
+        copy_to(piece(kind, t_f, 2), kind, FAR_L, left).wait_recv()
+        copy_to(piece(kind, t_f, 2), kind, ACROSS, other).start()
+
+    def slices(kind, count):
+        return (tok, tok, hid, hid)[kind].at[kind & 1, pl.ds(0, count)]
 
     def ag_end(kind):
-        for i, half in ((OWN_C, None), (C_L, None), (C_R, None), (C_F0, 0), (C_F1, 1)):
-            copy_to(piece(kind, t, half), kind, i, other).wait_recv()
+        ref = slices(kind, 4)
+        pltpu.make_async_copy(ref, ref, arecv.at[kind, ACROSS]).wait()
 
     def ag_drain(kind):
-        for i in (OWN_C, C_L, C_R):
-            copy_to(piece(kind, t, None), kind, i, other).wait_send()
-        for i in (OWN_R0, OWN_R1, OWN_L0, OWN_L1, FAR_R, FAR_L, C_F0, C_F1):
-            copy_to(piece(kind, t, 0), kind, i, other).wait_send()
+        ref = slices(kind, 7)
+        pltpu.make_async_copy(ref, ref, asend.at[kind]).wait()
 
     def send_tokens(p):
         for j, dz, lo, hi in PLANES:
             for dy in range(4):
-                if j in (1, 2) or (dz == 0 and dy == 0):
+                if j > 1 or (dz == 0 and dy == 0):
                     continue
                 gg, ff = at_zy(z + dz, y + dy)
                 pltpu.make_async_remote_copy(
-                    src_ref=slots_x.at[p, j // 3, (y + dy) & 3, pl.ds(lo, hi - lo)],
+                    src_ref=slots_x.at[p, j, (y + dy) & 3, pl.ds(lo, hi - lo)],
                     dst_ref=tok.at[p, t, j * 4 + y, pl.ds(lo, hi - lo)],
-                    send_sem=tsend.at[p],
-                    recv_sem=trecv.at[p],
+                    send_sem=tsend.at[0],
+                    recv_sem=trecv.at[p, j],
                     device_id=(gg, ff, t),
                     device_id_type=MESH,
                 ).start()
@@ -264,17 +269,17 @@
                 gg, ff = at_zy(z, y + dy)
                 pltpu.make_async_remote_copy(
                     src_ref=spread.at[d, p, (y + dy) & 3],
-                    dst_ref=tok.at[p, t, (d + 1) * 4 + y],
-                    send_sem=tsend.at[p],
-                    recv_sem=trecv.at[p],
+                    dst_ref=tok.at[p, t, (d + 2) * 4 + y],
+                    send_sem=tsend.at[0],
+                    recv_sem=trecv.at[p, 2],
                     device_id=(gg, ff, t),
                     device_id_type=MESH,
                 ).start()
-            tok[p, t, (d + 1) * 4 + y] = spread[d, p, y]
-
-    def await_tokens(sems, p):
-        part = tok.at[p, t, pl.ds(0, 13)]
-        pltpu.make_async_copy(part, part, sems.at[p]).wait()
+            tok[p, t, (d + 2) * 4 + y] = spread[d, p, y]
+
+    def await_tokens(sems, p, part):
+        ref = tok.at[p, t, pl.ds(0, (3, 4, 6)[part])]
+        pltpu.make_async_copy(ref, ref, sems.at[p, part]).wait()
 
     def back(p, sem):
         return (ans, ansa, ansb)[sem]
@@ -306,7 +311,7 @@
             pltpu.make_async_remote_copy(
                 src_ref=w_d.at[p, pl.ds(tt * 4, 4), pl.ds(32 * h, 32)],
                 dst_ref=dx.at[p, h, t],
-                send_sem=dsend.at[p, h],
+                send_sem=dsend.at[0],
                 recv_sem=drecv.at[p, h],
                 device_id=(g, f, tt),
                 device_id_type=MESH,
@@ -321,20 +326,23 @@
         pltpu.make_async_copy(part, part, sems.at[p, h]).wait()
 
     def hidden(p):
-        def body(r, carry):
-            rows = jnp.concatenate(
-                [tok[p, tt, pl.ds(r * 4, 4)].reshape(256, 256) for tt in range(8)], axis=1
-            )
+        for r in (2, 3, 0, 1):
+            rows = jnp.concatenate([tok[p, tt, pl.ds(r * 4, 4)].reshape(256, 256) for tt in range(8)], axis=1)
             pre = jnp.dot(rows, w_gu[p][...].reshape(2048, 256), preferred_element_type=F32) * 2048 ** (-0.5)
             gate, up = pre[:, 0:128], pre[:, 128:256]
             value = gate / (1.0 + jnp.exp(-gate)) * up
             hid[p, t, pl.ds(r * 256, 256)] = value.astype(BF)
-            return carry
-
-        lax.fori_loop(0, 4, body, 0)
+            if r == 3:
+                own_left(HID0 + p, 2)
+            elif r < 2:
+                own_right(HID0 + p, r)
+        own_right(HID0 + p, 2)
+        own_left(HID0 + p, 0)
+        own_left(HID0 + p, 1)
+        own_other(HID0 + p)
 
     def expert_out(p, halves, sem, lanes):
-        for r in (3, 1, 2, 0):
+        for r in (1, 2, 3, 0):
             rows = jnp.concatenate([hid[p, tt, pl.ds(r * 256, 256)] for tt in range(8)], axis=1)
             cols = jnp.concatenate(
                 [
@@ -444,6 +452,10 @@
     round_gu(0, gain)
     send_w(stage_gu.at[0], w_gu0, 2, all_rows, 1, 8, 4)
     round_gu(1, gain)
+    for p in range(2):
+        await_tokens(trecv, p, 0)
+        own_right(p, 0)
+        own_left(p, 0)
     pass_near(0)
     pass_near(1)
     send_w_other(stage_gu.at[0], w_gu0, 2)
@@ -452,10 +464,21 @@
     round_d(1)
     send_w(stage_d.at[1], w_d.at[1], 1, rows_a)
     send_w(stage_d.at[1], w_d.at[1], 4, rows_b)
-    await_tokens(trecv, 0)
-    ag_own(TOK0)
-    await_tokens(trecv, 1)
-    ag_own(TOK1)
+    for p in range(2):
+        await_tokens(trecv, p, 1)
+        own_right(p, 1)
+        own_left(p, 1)
+    relay_right(TOK0, 0)
+    await_tokens(trecv, 0, 2)
+    own_left(TOK0, 2)
+    own_right(TOK0, 2)
+    own_other(TOK0)
+    relay_right(TOK1, 0)
+    await_tokens(trecv, 1, 2)
+    own_left(TOK1, 2)
+    own_right(TOK1, 2)
+    own_other(TOK1)
+    relay_right(TOK0, 1)
     loads[6].wait()
     slot0 = column(slot0_row)
     slot1 = column(slot1_row)
@@ -469,25 +492,28 @@
             upper = weight.astype(BF)
             (hi0, hi1)[p][:, cols] = upper
             (lo0, lo1)[p][:, cols] = (weight - upper.astype(F32)).astype(BF)
-    ag_relay(TOK0)
+    relay_right(TOK1, 1)
+    relay_left(TOK0)
     ag_pass(TOK0)
-    ag_relay(TOK1)
+    relay_left(TOK1)
+    ag_pass(TOK1)
     ag_far(TOK0)
-    ag_pass(TOK1)
-    ag_far(TOK1)
     ag_end(TOK0)
     await_w(wrecv, w_gu0, 2, all_rows)
     hidden(0)
-    ag_own(HID0)
+    ag_far(TOK1)
     ag_end(TOK1)
-    ag_relay(HID0)
+    relay_left(HID0)
+    relay_right(HID0, 0)
+    relay_right(HID0, 1)
     ag_pass(HID0)
     ag_far(HID0)
     ag_end(HID0)
     await_w(wrecv, w_gu1, 3, all_rows)
     hidden(1)
-    ag_own(HID1)
-    ag_relay(HID1)
+    relay_left(HID1)
+    relay_right(HID1, 0)
+    relay_right(HID1, 1)
     ag_pass(HID1)
     await_w(wrecv, w_d.at[0], 0, all_rows)
     send_dx(0, 0)
@@ -510,10 +536,8 @@
     for d in range(2):
         for cp in near_copies(d):
             cp.wait_send()
-    for p in range(2):
-        await_tokens(tsend, p)
-        for h in range(2):
-            await_dx(dsend, p, h)
+    for ref, sem in ((tok.at[0, pl.ds(0, 2), pl.ds(0, 13)], tsend), (dx.at[:, :, pl.ds(0, 7)], dsend)):
+        pltpu.make_async_copy(ref, ref, sem.at[0]).wait()
     await_w(wsend, w_d.at[0], 0, all_rows)
     await_w(wsend, w_d.at[1], 1, rows_a)
     await_w(wsend, w_gu0, 2, all_rows)
@@ -611,13 +635,13 @@
             dma((7,)),
             dma((5,)),
             dma((5,)),
-            dma((2,)),
-            dma((2,)),
+            dma((1,)),
+            dma((2, 3)),
             dma((2, 2)),
             dma((2, 2)),
-            dma((4, 11)),
-            dma((4, 11)),
-            dma((2, 2)),
+            dma((4,)),
+            dma((4, 8)),
+            dma((1,)),
             dma((2, 2)),
             dma((3,)),
             dma((3,)),

time: 110 us -> 108 us (0.982)
  Pallas kernels: 109 us -> 107 us
    pallas_call x1, Pallas kernels: 107 us -> 105 us  [per_device(): pl.pallas_call(kernel, out_shape=(both, both, ready, select, select, tota...]
where the time goes in v6:
time: 108 us
  Pallas kernels  107 us (99%)
    pallas_call x1, Pallas kernels, per_device(): pl.pallas_call(kernel, out_shape=(both, both, ready, select, select, tota...  105 us
    pallas_call x1, Pallas kernels, per_device(): pl.pallas_call(copy_out, out_shape=(ready, ready, ready, block), in_specs...  2.45 us

profile of v6, /device:TPU:1, one launch (start us, length us, event | category | flops | bytes accessed | tf_op | source)
XLA Modules:
  0.0 107.8 jit_solution(15409531339511938947)
XLA Ops:
  0.6 104.7 %shard_map.102 = (bf16[32,64,256]{2,1,0:T(8,128)(2,1)S(1)}, bf16[32,64,256]{2,1,0:T(8,128)(2,1)S(1)}, bf16[2,32,64,128]{3,2,1,0:T(8,128)(2,1)S(1)}, bf16[512,102...) custom-call(bf16[512,2048]{1,0:T(8,128)(2,1)} %prompt_hbm.1, ...), custom_call_target="tpu_custom_call" | custom-call | tf_op jit(solution)/shard_map/pallas_call | solution.py:606
  105.3 2.4 %shard_map.103 = (bf16[2,32,64,128]{3,2,1,0:T(8,128)(2,1)}, bf16[2,32,64,128]{3,2,1,0:T(8,128)(2,1)}, bf16[2,32,64,128]{3,2,1,0:T(8,128)(2,1)}, bf16[512,256]{1,0:T(8,128)(2,1)}) custom-call(bf16[32,64,256]{2,1,0:T(8,128)(2,1)S(1)} %get-tuple-element.15.w_gu0, bf16[32,64,256]{2,1,0:T(8,128)(2,1)S(1)} %get-tuple-element.16.w_gu1, ...), custom_call_target="tpu_custom_call" | custom-call | tf_op jit(solution)/shard_map/pallas_call | solution.py:666

commit v7 on v6

--- a/solution.py
+++ b/solution.py
@@ -574,7 +574,8 @@
         pltpu.make_async_copy(w_gu0.at[:, :, pl.ds(128, 128)], up_out.at[0], sem.at[2]),
         pltpu.make_async_copy(w_gu1.at[:, :, pl.ds(128, 128)], up_out.at[1], sem.at[3]),
         pltpu.make_async_copy(w_d, down_out, sem.at[4]),
-        pltpu.make_async_copy(blend_v, blend_out, sem.at[5]),
+        pltpu.make_async_copy(blend_v.at[pl.ds(0, 256)], blend_out.at[pl.ds(0, 256)], sem.at[5]),
+        pltpu.make_async_copy(blend_v.at[pl.ds(256, 256)], blend_out.at[pl.ds(256, 256)], sem.at[6]),
     ]
     for cp in copies[:5]:
         cp.start()
@@ -583,11 +584,13 @@
     goes = a == ((b >> 5) & 1) * 128 + (b >> 6) * 32 + (b & 31)
     to_place = jnp.where(goes, 1.0, 0.0).astype(BF)
     values = ansb[...].reshape(1024, 128)
-    part = jnp.dot(hi1[...], values, preferred_element_type=F32)
-    part += jnp.dot(lo1[...], values, preferred_element_type=F32)
-    total = jnp.concatenate([acc[:, 0:128], acc[:, 128:256] + part], axis=1).astype(BF)
-    blend_v[...] = jnp.dot(total, to_place, preferred_element_type=F32).astype(BF)
-    copies[5].start()
+    for r in range(2):
+        rows = pl.ds(r * 256, 256)
+        part = jnp.dot(hi1[rows], values, preferred_element_type=F32)
+        part += jnp.dot(lo1[rows], values, preferred_element_type=F32)
+        total = jnp.concatenate([acc[rows, 0:128], acc[rows, 128:256] + part], axis=1).astype(BF)
+        blend_v[rows] = jnp.dot(total, to_place, preferred_element_type=F32).astype(BF)
+        copies[5 + r].start()
     for cp in copies:
         cp.wait()
 
@@ -668,7 +671,7 @@
         out_shape=(ready, ready, ready, block),
         in_specs=[vmem] * 7,
         out_specs=(hbm,) * 4,
-        scratch_shapes=[pltpu.VMEM((512, 256), BF), dma((6,))],
+        scratch_shapes=[pltpu.VMEM((512, 256), BF), dma((7,))],
         compiler_params=pltpu.CompilerParams(vmem_limit_bytes=16 * 2**20),
     )(*passed)
     flat = lambda a: a.reshape(2, 2048, 128)

time: 108 us -> 107 us (level)
  no operation moved by 1% of the time
where the time goes in v7:
time: 107 us
  Pallas kernels  107 us (100%)
    pallas_call x1, Pallas kernels, per_device(): pl.pallas_call(kernel, out_shape=(both, both, ready, select, select, tota...  105 us

profile of v7, /device:TPU:1, one launch (start us, length us, event | category | flops | bytes accessed | tf_op | source)
XLA Modules:
  0.0 107.2 jit_solution(3084740091556762682)
XLA Ops:
  0.6 104.7 %shard_map.102 = (bf16[32,64,256]{2,1,0:T(8,128)(2,1)S(1)}, bf16[32,64,256]{2,1,0:T(8,128)(2,1)S(1)}, bf16[2,32,64,128]{3,2,1,0:T(8,128)(2,1)S(1)}, bf16[512,102...) custom-call(bf16[512,2048]{1,0:T(8,128)(2,1)} %prompt_hbm.1, ...), custom_call_target="tpu_custom_call" | custom-call | tf_op jit(solution)/shard_map/pallas_call | solution.py:609
  105.3 1.9 %shard_map.103 = (bf16[2,32,64,128]{3,2,1,0:T(8,128)(2,1)}, bf16[2,32,64,128]{3,2,1,0:T(8,128)(2,1)}, bf16[2,32,64,128]{3,2,1,0:T(8,128)(2,1)}, bf16[512,256]{1,0:T(8,128)(2,1)}) custom-call(bf16[32,64,256]{2,1,0:T(8,128)(2,1)S(1)} %get-tuple-element.15.w_gu0, bf16[32,64,256]{2,1,0:T(8,128)(2,1)S(1)} %get-tuple-element.16.w_gu1, ...), custom_call_target="tpu_custom_call" | custom-call | tf_op jit(solution)/shard_map/pallas_call | solution.py:669
